TPU v7x, 32 devices: a whole 2x2x4 slice. The times are simulated.
32 devices in a mesh: grp: 2 (over y), sp: 4 (over z), tp: 4 (over x, core).
Axes of the slice: x: 2, y: 2, z: 4, core: 2. Of those that a mesh axis runs over, the one named last changes fastest.
Arguments:
- latent: bfloat16 [4096, 2048], P(('grp', 'sp', 'tp')), parts along dimension 0, may hold values from -3 to 3
- context: bfloat16 [1024, 2048], P(('grp', 'sp')), parts along dimension 0, may hold values from -6 to 6
- condition: float32 [4096], P(('grp', 'sp')), parts along dimension 0, may hold values from -6 to 6
- context_condition: float32 [2048], P('sp'), may hold values from -6 to 6
- mod_weight: bfloat16 [2048, 6144], P('sp', 'tp'), may hold values from -0.1875 to 0.1875
- mod_bias: float32 [6144], replicated, may hold values from -1.5 to 1.5
- query_weight: bfloat16 [2048, 1024], P('sp'), may hold values from -0.125 to 0.125
- key_weight: bfloat16 [2048, 1024], P('sp'), may hold values from -0.125 to 0.125
- value_weight: bfloat16 [2048, 2048], P(None, 'tp'), may hold values from -3 to 3
- out_gate_weight: bfloat16 [2048, 2048], P(None, 'tp'), may hold values from -0.125 to 0.125
- decay_in_weight: bfloat16 [2048, 32], replicated, may hold values from -0.125 to 0.125
- decay_weight: bfloat16 [2, 16, 1024], replicated, may hold values from -1.5 to 1.5
- decay_bias: float32 [2, 1024], replicated, may hold values from 0.5 to 11
- extra_decay: float32 [2, 4, 2048], P(None, None, 'sp'), may hold values from -2.1 to 0
- norm_gain: float32 [512], replicated, may hold values from 0.1 to 1.9
- out_weight: bfloat16 [2048, 2048], P('tp'), may hold values from -0.25 to 0.25
- final_gain: float32 [2048], replicated, may hold values from 0.1 to 1.9
- final_bias: float32 [2048], replicated, may hold values from -1.5 to 1.5
Outputs:
- output: bfloat16 [4096, 2048], P(('grp', 'sp', 'tp')), parts along dimension 0
There are 2 independent parts, one for each index of `grp`. A program takes and returns all parts, laid end to end along the dimension named above; an argument that names none is the same for every part. Nothing has to cross between parts.
All inputs are finite; a program needn't handle non-finite values.
Results may differ from a plain program's by a relative error of at most 0.012.
The roundings to bfloat16 on the way count: a program that leaves them out, or rounds other values in their place, can miss the bound.
Values may be sent and summed in bfloat16 or wider, within the bound.
A program may use at most 64 MiB of HBM per device.

v0:
```python
import functools

import jax
import jax.numpy as jnp
from jax import lax
from jax.experimental import pallas as pl
from jax.experimental.pallas import tpu as pltpu
from jax.sharding import PartitionSpec as P

ATTENTION_HEADS = 4
DV = 512
BLOCK = 64
GRID_W = 64


norm_eps = 1e-05
gate_scale = 16.0
rope_base = 10000.0
residual_scale = 2.0**0.5
highest = lax.Precision.HIGHEST
f32 = jnp.float32
bf16 = jnp.bfloat16


def rope_tables(token_places, width):
    quarter = width // 4
    frequency = rope_base ** (-jnp.arange(quarter, dtype=f32) / quarter)
    row_angle = (token_places // GRID_W).astype(f32)[:, None] * frequency
    col_angle = (token_places % GRID_W).astype(f32)[:, None] * frequency
    cosine = jnp.concatenate([jnp.cos(row_angle)] * 2 + [jnp.cos(col_angle)] * 2, axis=1)
    row_sine, col_sine = jnp.sin(row_angle), jnp.sin(col_angle)
    sine = jnp.concatenate([-row_sine, row_sine, -col_sine, col_sine], axis=1)
    return cosine, sine


def dot(a, b, contract=((1,), (0,)), precision=None):
    return lax.dot_general(a, b, (contract, ((), ())), precision=precision,
                           preferred_element_type=f32)


def log_sigmoid(x):
    return jnp.minimum(x, 0.0) - jnp.log1p(jnp.exp(-jnp.abs(x)))


def rotate(x, cosine, sine):
    half = x.shape[1] // 2
    parts = [pltpu.roll(x[:, i * half:(i + 1) * half], half // 2, 1) for i in range(2)]
    return x * cosine + jnp.concatenate(parts, axis=1) * sine


def triangle(size, reverse):
    row = lax.broadcasted_iota(jnp.int32, (size, size), 0)
    col = lax.broadcasted_iota(jnp.int32, (size, size), 1)
    return row <= col if reverse else row >= col


def decay_block(low, decay_weight, decay_bias, direction):
    rank = decay_weight.shape[1]
    logits = dot(low[:, direction * rank:(direction + 1) * rank], decay_weight[direction])
    return log_sigmoid(logits + decay_bias[direction:direction + 1, :]) / gate_scale


def context_kernel(k_ref, v_ref, low_ref, dw_ref, db_ref, state_ref):
    length, width = k_ref.shape
    size = min(2 * BLOCK, length)
    count = length // size
    for direction in range(2):
        mask = triangle(size, direction == 1).astype(f32)
        edge = 0 if direction == 1 else size - 1
        state = None
        for step in range(count):
            b = count - 1 - step if direction == 1 else step
            rows = slice(b * size, (b + 1) * size)
            logdec = decay_block(low_ref[rows, :], dw_ref[...], db_ref[...], direction)
            cum = dot(mask, logdec, precision=highest)
            total = cum[edge:edge + 1, :]
            closing = (k_ref[rows, :].astype(f32) * jnp.exp(total - cum)).astype(bf16)
            term = dot(closing, v_ref[rows, :], ((0,), (0,)))
            state = term if state is None else jnp.exp(total).T * state + term
        state_ref[direction] = state


def local_kernel(q_ref, k_ref, v_ref, low_ref, extra_ref, dw_ref, db_ref, cos_ref, sin_ref,
                 out_ref, qc_ref, state_ref, total_ref):
    length, width = q_ref.shape
    size = 2 * BLOCK
    count = length // size
    rq, rk, within, scores = [], [], [], []
    for b in range(count):
        rows = slice(b * size, (b + 1) * size)
        cosine, sine = cos_ref[rows, :], sin_ref[rows, :]
        rq.append(rotate(q_ref[rows, :].astype(f32) * width ** -0.5, cosine, sine))
        rk.append(rotate(k_ref[rows, :].astype(f32), cosine, sine))
        scores.append(None)
    for direction in range(2):
        keep = triangle(size, direction == 1)
        mask = keep.astype(f32)
        edge = 0 if direction == 1 else size - 1
        middle = size // 2 if direction == 1 else size // 2 - 1
        state = None
        before = None
        for step in range(count):
            b = count - 1 - step if direction == 1 else step
            rows = slice(b * size, (b + 1) * size)
            logdec = decay_block(low_ref[rows, :], dw_ref[...], db_ref[...], direction)
            logdec = logdec + extra_ref[rows, direction:direction + 1]
            cum = dot(mask, logdec, precision=highest)
            total = cum[edge:edge + 1, :]
            center = cum[middle:middle + 1, :]
            q_mid = (rq[b] * jnp.exp(cum - center)).astype(bf16)
            k_mid = (rk[b] * jnp.exp(center - cum)).astype(bf16)
            score = jnp.where(keep, dot(q_mid, k_mid, ((1,), (1,))), 0.0)
            q_dec = rq[b] * jnp.exp(cum)
            if direction == 0:
                scores[b] = score
                out = None
            else:
                out = dot((scores[b] + score).astype(bf16), v_ref[rows, :])
            if state is not None:
                carried = dot(q_dec.astype(bf16), state.astype(bf16))
                out = carried if out is None else out + carried
            if direction == 0:
                out_ref[rows, :] = jnp.zeros((size, v_ref.shape[1]), f32) if out is None else out
            else:
                out_ref[rows, :] += out
            q_all = q_dec if before is None else q_dec * jnp.exp(before)
            qc_ref[rows, direction * width:(direction + 1) * width] = q_all.astype(bf16)
            closing = (rk[b] * jnp.exp(total - cum)).astype(bf16)
            term = dot(closing, v_ref[rows, :], ((0,), (0,)))
            state = term if state is None else jnp.exp(total).T * state + term
            before = total if before is None else before + total
        state_ref[direction * width:(direction + 1) * width, :] = state.astype(bf16)
        total_ref[direction:direction + 1, :] = before


def join_kernel(final, out_ref, qc_ref, states_ref, totals_ref, start_ref, gate_ref, gain_ref,
                place_ref, result_ref):
    count = states_ref.shape[0]
    width = qc_ref.shape[1] // 2
    place = place_ref[...]
    mixture = out_ref[...]
    for direction in range(2):
        state = start_ref[direction]
        for lap in range(count):
            j = count - 1 - lap if direction == 1 else lap
            decay = jnp.exp(totals_ref[j, direction:direction + 1, :]).T
            joined = decay * state + states_ref[
                j, direction * width:(direction + 1) * width, :].astype(f32)
            ahead = place < j if direction == 1 else place > j
            state = jnp.where(ahead, joined, state)
        mixture = mixture + dot(qc_ref[:, direction * width:(direction + 1) * width],
                                state.astype(bf16))
    if final:
        squares = jnp.mean(mixture * mixture, axis=1, keepdims=True)
        gate = gate_ref[...].astype(f32)
        normed = mixture * lax.rsqrt(squares + norm_eps) * gain_ref[...]
        result_ref[...] = (normed * (gate / (1.0 + jnp.exp(-gate)))).astype(bf16)
    else:
        result_ref[...] = mixture


def call(kernel, out_shape, *args):
    return pl.pallas_call(
        kernel,
        out_shape=out_shape,
        in_specs=[pl.BlockSpec(memory_space=pltpu.VMEM)] * len(args),
        out_specs=jax.tree.map(lambda _: pl.BlockSpec(memory_space=pltpu.VMEM), out_shape),
        compiler_params=pltpu.CompilerParams(vmem_limit_bytes=48 * 1024 * 1024),
        cost_estimate=pl.CostEstimate(flops=4_000_000_000, bytes_accessed=4_000_000,
                                      transcendentals=1_000_000),
    )(*args)


MESH = pl.DeviceIdType.MESH


def remote(src, dst, send_sem, recv_sem, axis, target):
    return pltpu.make_async_remote_copy(
        src_ref=src, dst_ref=dst, send_sem=send_sem, recv_sem=recv_sem,
        device_id={axis: target}, device_id_type=MESH)


class Line:
    def __init__(self, place, count, axis, target_of, view, chunks, send_sem, recv_sem):
        self.place, self.count, self.axis, self.target_of = place, count, axis, target_of
        self.view, self.chunks, self.send_sem, self.recv_sem = view, chunks, send_sem, recv_sem

    def copy(self, way, hop, chunk, block, target):
        ref = self.view(block, chunk)
        return remote(ref, ref, self.send_sem.at[way, hop, chunk],
                      self.recv_sem.at[way, hop, chunk], self.axis, self.target_of(target))

    def outgoing(self, way, hop):
        place, count = self.place, self.count
        if way == 0:
            return place - hop, place + 1, jnp.logical_and(place >= hop, place < count - 1)
        return place + hop, place - 1, jnp.logical_and(place + hop < count, place > 0)

    def each_send(self, way, hop, chunk, act):
        block, target, valid = self.outgoing(way, hop)

        @pl.when(valid)
        def _():
            act(self.copy(way, hop, chunk, block, target))

    def send(self, way, hop, chunk):
        self.each_send(way, hop, chunk, lambda c: c.start())

    def drain(self):
        for way in range(2):
            for hop in range(self.count - 1):
                for chunk in range(self.chunks):
                    self.each_send(way, hop, chunk, lambda c: c.wait_send())

    def arrive(self, way, hop, chunk, then=None):
        if way == 0:
            block, source, valid = self.place - 1 - hop, self.place - 1, self.place > hop
        else:
            block, source = self.place + 1 + hop, self.place + 1
            valid = self.place + 1 + hop < self.count

        @pl.when(valid)
        def _():
            self.copy(way, hop, chunk, block, source).wait_recv()
            if then is not None:
                then(block)

    def forward(self, hop, then=None):
        for chunk in range(self.chunks):
            for way in range(2):
                self.arrive(way, hop, chunk, None if then is None else functools.partial(then, way))
                if hop + 1 < self.count - 1:
                    self.send(way, hop + 1, chunk)


def open_kernel(partners):
    barrier = pltpu.get_barrier_semaphore()
    for axis, target in partners:
        pl.semaphore_signal(barrier, inc=1, device_id={axis: target}, device_id_type=MESH)
    return lambda: pl.semaphore_wait(barrier, len(partners))


def others(axis):
    count, place = lax.axis_size(axis), lax.axis_index(axis)
    return [lax.rem(place + k, count) for k in range(1, count)]


def sources(axis):
    count, place = lax.axis_size(axis), lax.axis_index(axis)
    return [lax.rem(place + count - k, count) for k in range(1, count)]


def spread(buffer, axis, send_sem, recv_sem):
    place = lax.axis_index(axis)
    for k, target in enumerate(others(axis)):
        remote(buffer.at[place], buffer.at[place], send_sem.at[k], recv_sem.at[k],
               axis, target).start()


def spread_arrive(buffer, axis, send_sem, recv_sem):
    for k, source in enumerate(sources(axis)):
        remote(buffer.at[source], buffer.at[source], send_sem.at[k], recv_sem.at[k],
               axis, source).wait_recv()


def spread_drain(buffer, axis, send_sem, recv_sem):
    place = lax.axis_index(axis)
    for k, target in enumerate(others(axis)):
        remote(buffer.at[place], buffer.at[place], send_sem.at[k], recv_sem.at[k],
               axis, target).wait_send()


def enter_kernel(chunks, latent_ref, context_ref, cond_ref, mw_ref, mb_ref, qw_ref, kw_ref,
                 ml_ref, mc_ref, gate_ref, qk_ref,
                 rows_ref, part_ref, sums_ref, zs, zr, xs, xr, cs, cr, ps, pr, ss, sr):
    sp, sp_count = lax.axis_index("sp"), lax.axis_size("sp")
    tp, tp_count = lax.axis_index("tp"), lax.axis_size("tp")
    own, model_width = latent_ref.shape
    depth = qw_ref.shape[0]
    head_keys = qk_ref.shape[1] // 2
    ready = open_kernel([("sp", t) for t in others("sp")] + [("tp", t) for t in others("tp")])
    v = cond_ref[...]
    activated = (v / (1.0 + jnp.exp(-v))).astype(bf16)
    part_ref[sp] = dot(activated, mw_ref[...])
    columns = pl.ds(pl.multiple_of((tp // (tp_count // ATTENTION_HEADS)) * head_keys, head_keys),
                    head_keys)
    qk_rows = pl.ds(pl.multiple_of(sp * depth, depth), depth)
    qk_ref[qk_rows, :head_keys] = qw_ref[:, columns]
    qk_ref[qk_rows, head_keys:] = kw_ref[:, columns]
    rows_ref[pl.ds(pl.multiple_of(tp * own, own), own), :] = latent_ref[...]

    step = depth // chunks
    z_line = Line(
        sp, sp_count, "sp", lambda p: p,
        lambda block, chunk: qk_ref.at[
            pl.ds(pl.multiple_of(block * depth + chunk * step, step), step), :],
        chunks, zs, zr)
    x_count = tp_count // 2
    x, core = tp // 2, tp % 2

    def rows_of(block, chunk):
        return rows_ref.at[pl.ds(pl.multiple_of((2 * block + core) * own, own), own), :]

    x_line = Line(x, x_count, "tp", lambda p: 2 * p + core, rows_of, 1, xs, xr)
    sibling = tp + 1 - 2 * core

    def cross(block, slot, other=False):
        side = 1 - core if other else core
        ref = rows_ref.at[pl.ds(pl.multiple_of((2 * block + side) * own, own), own), :]
        return remote(ref, ref, cs.at[slot], cr.at[slot], "tp", sibling)

    def slot_of(way, hop):
        return 1 + way * (x_count - 1) + hop

    ready()
    spread(part_ref, "sp", ps, pr)
    for way in range(2):
        x_line.send(way, 0, 0)
    cross(x, 0).start()
    for chunk in range(chunks):
        for way in range(2):
            z_line.send(way, 0, chunk)
    spread_arrive(part_ref, "sp", ps, pr)
    total = part_ref[0]
    for j in range(1, sp_count):
        total = total + part_ref[j]
    sums_ref[tp] = total
    spread(sums_ref, "tp", ss, sr)
    z_line.forward(0)
    for hop in range(x_count - 1):
        x_line.forward(hop, lambda way, block, hop=hop: cross(block, slot_of(way, hop)).start())
    if sp_count > 2:
        z_line.forward(1)
    spread_arrive(sums_ref, "tp", ss, sr)
    modulation = jnp.concatenate([sums_ref[j] for j in range(tp_count)], axis=1) + mb_ref[...]
    shifts = modulation[:, :model_width]
    scales = modulation[:, model_width:2 * model_width]
    gate_ref[...] = modulation[0:1, 2 * model_width:]
    mc_ref[...] = (context_ref[...].astype(f32) * (1.0 + scales[1:2]) + shifts[1:2]).astype(bf16)

    def each_cross(act_own, act_line):
        act_own()
        for way in range(2):
            for hop in range(x_count - 1):
                block = x - 1 - hop if way == 0 else x + 1 + hop
                valid = x > hop if way == 0 else x + 1 + hop < x_count

                @pl.when(valid)
                def _():
                    act_line(block, slot_of(way, hop))

    each_cross(lambda: cross(x, 0, True).wait_recv(),
               lambda block, slot: cross(block, slot, True).wait_recv())
    for j in range(tp_count):
        rows = slice(j * own, (j + 1) * own)
        ml_ref[rows, :] = (rows_ref[rows, :].astype(f32) * (1.0 + scales[0:1])
                           + shifts[0:1]).astype(bf16)
    for hop in range(2, sp_count - 1):
        z_line.forward(hop)
    each_cross(lambda: cross(x, 0).wait_send(),
               lambda block, slot: cross(block, slot).wait_send())
    spread_drain(part_ref, "sp", ps, pr)
    spread_drain(sums_ref, "tp", ss, sr)
    x_line.drain()
    z_line.drain()


def comm_call(kernel, out_shape, scratch, collective_id, *args):
    return pl.pallas_call(
        kernel,
        out_shape=out_shape,
        in_specs=[pl.BlockSpec(memory_space=pltpu.VMEM)] * len(args),
        out_specs=jax.tree.map(lambda _: pl.BlockSpec(memory_space=pltpu.VMEM), out_shape),
        scratch_shapes=scratch,
        compiler_params=pltpu.CompilerParams(
            vmem_limit_bytes=48 * 1024 * 1024, collective_id=collective_id,
            has_side_effects=True),
        cost_estimate=pl.CostEstimate(flops=20_000_000_000, bytes_accessed=60_000_000,
                                      transcendentals=1_000_000),
    )(*args)


def enter(latent, context, cond, mod_weight, mod_bias, query_weight, key_weight):
    sp_count, tp_count = lax.axis_size("sp"), lax.axis_size("tp")
    own, model_width = latent.shape
    depth = query_weight.shape[0]
    head_keys = query_weight.shape[1] // ATTENTION_HEADS
    chunks = 4
    sds = jax.ShapeDtypeStruct
    dma = pltpu.SemaphoreType.DMA
    x_hops = tp_count // 2 - 1
    return comm_call(
        functools.partial(enter_kernel, chunks),
        (
            sds((own * tp_count, model_width), bf16),
            sds(context.shape, bf16),
            sds((1, model_width), f32),
            sds((depth * sp_count, 2 * head_keys), bf16),
        ),
        [
            pltpu.VMEM((own * tp_count, model_width), bf16),
            pltpu.VMEM((sp_count, 2, mod_weight.shape[1]), f32),
            pltpu.VMEM((tp_count, 2, mod_weight.shape[1]), f32),
            dma((2, sp_count - 1, chunks)), dma((2, sp_count - 1, chunks)),
            dma((2, x_hops, 1)), dma((2, x_hops, 1)),
            dma((1 + 2 * x_hops,)), dma((1 + 2 * x_hops,)),
            dma((sp_count - 1,)), dma((sp_count - 1,)),
            dma((tp_count - 1,)), dma((tp_count - 1,)),
        ],
        1, latent, context, cond, mod_weight, mod_bias[None, :], query_weight, key_weight,
    )


def project(rows, weight):
    return jnp.dot(rows, weight, preferred_element_type=f32).astype(bf16)


def body(
    latent,
    context,
    condition,
    context_condition,
    mod_weight,
    mod_bias,
    query_weight,
    key_weight,
    value_weight,
    out_gate_weight,
    decay_in_weight,
    decay_weight,
    decay_bias,
    extra_decay,
    norm_gain,
    out_weight,
    final_gain,
    final_bias,
):
    head_keys = query_weight.shape[1] // ATTENTION_HEADS
    value_cols = value_weight.shape[1]
    tp_index = lax.axis_index("tp")
    sp_index = lax.axis_index("sp")
    head_share = lax.axis_size("tp") // ATTENTION_HEADS
    head_index = tp_index // head_share
    part_index = tp_index % head_share
    key_start = head_index * head_keys

    full_out = lax.all_gather(out_weight, "tp", axis=0, tiled=True)
    mod_latent, mod_context, branch_gate, qk_head = enter(
        latent, context, jnp.stack([condition, context_condition]), mod_weight, mod_bias,
        query_weight, key_weight,
    )
    context_local = jnp.concatenate(
        [
            project(mod_context, qk_head[:, head_keys:]),
            project(mod_context, value_weight),
            project(mod_context, decay_in_weight),
        ],
        axis=1,
    )
    gathered_context = lax.all_gather(context_local, "sp", axis=0, tiled=True)
    qk = project(mod_latent, qk_head)
    value_rows = project(mod_latent, value_weight)
    out_gate = project(mod_latent, out_gate_weight)
    low_rank = project(mod_latent, decay_in_weight)
    count = mod_latent.shape[0]
    token_places = sp_index * count + jnp.arange(count, dtype=jnp.int32)
    cosine, sine = rope_tables(token_places, head_keys)
    head_bias = lax.dynamic_slice_in_dim(decay_bias, key_start, head_keys, 1)
    head_gate = lax.dynamic_slice_in_dim(decay_weight, key_start, head_keys, 2)
    head_extra = lax.dynamic_index_in_dim(extra_decay, head_index, 1, keepdims=False).T

    sds = jax.ShapeDtypeStruct
    out_local, qc, states, totals = call(
        local_kernel,
        (
            sds((count, value_cols), f32),
            sds((count, 2 * head_keys), bf16),
            sds((2 * head_keys, value_cols), bf16),
            sds((2, head_keys), f32),
        ),
        qk[:, :head_keys], qk[:, head_keys:], value_rows, low_rank, head_extra, head_gate,
        head_bias, cosine, sine,
    )
    start = call(
        context_kernel,
        sds((2, head_keys, value_cols), f32),
        gathered_context[:, :head_keys],
        gathered_context[:, head_keys : head_keys + value_cols],
        gathered_context[:, head_keys + value_cols :],
        head_gate, head_bias,
    )
    states, totals, full_out = lax.optimization_barrier((states, totals, full_out))
    all_states = lax.all_gather(states, "sp")
    all_totals = lax.all_gather(totals, "sp")
    place = jnp.full((1, value_cols), sp_index, jnp.int32)
    gain_slice = lax.dynamic_slice_in_dim(norm_gain, part_index * value_cols, value_cols, 0)
    final = head_share == 1
    joined = call(
        functools.partial(join_kernel, final),
        sds((count, value_cols), bf16 if final else f32),
        out_local, qc, all_states, all_totals, start, out_gate, gain_slice[None, :], place,
    )
    if final:
        gated_rows = joined
    else:
        squares = jnp.sum(joined * joined, axis=1)
        onehot = (jnp.arange(ATTENTION_HEADS) == head_index).astype(f32)
        sums = lax.psum(onehot[:, None] * squares[None, :], "tp")
        head_sum = jnp.sum(sums * onehot[:, None], axis=0)
        normed = joined * lax.rsqrt(head_sum / DV + norm_eps)[:, None] * gain_slice
        gated_rows = (normed * jax.nn.silu(out_gate.astype(f32))).astype(bf16)
    regrouped = lax.all_to_all(gated_rows, "tp", split_axis=0, concat_axis=1, tiled=True)
    branch = jnp.dot(regrouped, full_out, preferred_element_type=f32)
    summed = residual_scale * latent.astype(f32) + branch_gate * branch
    row_mean = jnp.mean(summed, axis=1, keepdims=True)
    centered = summed - row_mean
    variance = jnp.mean(centered * centered, axis=1, keepdims=True)
    return (centered * lax.rsqrt(variance + norm_eps) * final_gain + final_bias).astype(bf16)


def solution(mesh):
    placed = (
        P(("grp", "sp", "tp"), None),
        P(("grp", "sp"), None),
        P(("grp", "sp")),
        P("sp"),
        P("sp", "tp"),
        P(),
        P("sp", None),
        P("sp", None),
        P(None, "tp"),
        P(None, "tp"),
        P(),
        P(),
        P(),
        P(None, None, "sp"),
        P(),
        P("tp", None),
        P(),
        P(),
    )
    return jax.shard_map(
        body, mesh=mesh, in_specs=placed, out_specs=P(("grp", "sp", "tp"), None), check_vma=False
    )
```

profile of v0, /device:TPU:0, one launch (start us, length us, event | category | flops | bytes accessed | tf_op | source)
XLA Modules:
  0.0 169.5 jit_solution(9268698283201737938)
XLA Ops:
  6.5 0.0 copy-start
  6.5 0.0 all-gather.6.cloned.1.call-start
  6.6 0.7 all-gather.6.cloned.1.call-update
  7.3 0.0 all-gather.8.cloned.1.call-start
  7.3 0.8 constant_dynamic-slice_fusion.2
  8.1 0.1 copy.30
  8.2 0.0 copy-done.28
  8.3 0.0 copy-done.29
  8.3 0.0 copy-done.1
  8.3 0.0 copy-done.14
  8.3 0.0 copy-start.10
  8.3 1.4 copy-done.10
  9.7 1.2 copy-done.11
  10.9 1.2 copy-done.12
  12.2 1.0 copy-done.13
  13.2 43.2 %shard_map.172 = (bf16[512,2048]{1,0:T(8,128)(2,1)}, bf16[128,2048]{1,0:T(8,128)(2,1)S(1)}, f32[1,2048]{1,0:T(1,128)S(1)}, bf16[2048,512]{1,0:T(8,128)(2,1)}) custom-call(bf16[128,2048]{1,0:T(8,128)(2,1)S(1)} %copy-done.1, bf16[128,2048]{1,0:T(8,128)(2,1)S(1)} %copy-done.13, f32[2,512]{1,0:T(2,128)S(1)} %pad_maximum_fusion.3.cond_ref, ...), custom_call_target="tpu_custom_call" | custom-call | flops 20000000000 | bytes 60000000 | tf_op jit(solution)/shard_map/pallas_call | solution.py:369
  56.4 0.0 copy-start.3
  56.4 0.6 copy-done.3
  57.0 0.0 copy-done.25
  57.0 2.9 %convolution_convert_fusion.5 = bf16[512,32]{0,1:T(8,128)(2,1)} fusion(bf16[512,2048]{1,0:T(8,128)(2,1)} %get-tuple-element.17, bf16[2048,32]{0,1:T(8,128)(2,1)S(1)} %copy-done.25), kind=kOutput, calls=%fused_computation.7 | convolution fusion | flops 67125248 | bytes 2260992 | tf_op jit(solution)/shard_map/dot_general | solution.py:415
  60.0 0.9 copy.31.low_ref
  60.9 0.7 constant_dynamic-slice_fusion.db_ref
  61.6 0.7 constant_dynamic-slice_fusion.1.dw_ref
  62.3 1.9 %fusion.2 = (f32[512,64]{1,0:T(8,128)S(1)}, f32[512,64]{1,0:T(8,128)S(1)}, f32[512,64]{1,0:T(8,128)S(1)}, f32[512,64]{1,0:T(8,128)S(1)}, f32[512,64]{1,0:T(8,128)S(1)}, /*index=5*/f32[512,64]{1,0:T(8,128)S(1)}) fusion(f32[64]{0:T(128)S(1)} %multiply_power_fusion, f32[512]{0:T(512)S(1)} %get-tuple-element.40, f32[512]{0:T(512)S(1)} %get-tuple-element.41), kind=kLoop, calls=%fused_computation.19 | loop fusion | flops 131072 | bytes 790784 | tf_op jit(solution)/shard_map/neg | solution.py:32
  64.2 0.3 pad_maximum_fusion.cos_ref
  64.5 0.3 pad_maximum_fusion.1.sin_ref
  64.8 1.2 convolution_convert_fusion.2
  66.1 1.2 convolution_convert_fusion.1.v_ref
  67.3 5.6 %shard_map.173 = (f32[512,512]{1,0:T(8,128)S(1)}, bf16[512,512]{1,0:T(8,128)(2,1)S(1)}, bf16[512,512]{1,0:T(8,128)(2,1)S(1)}, f32[2,256]{1,0:T(2,128)S(1)}) custom-call(bf16[512,256]{1,0:T(8,128)(2,1)S(1)} %get-tuple-element.28.q_ref, bf16[512,256]{1,0:T(8,128)(2,1)S(1)} %get-tuple-element.27.k_ref, bf16[512,512]{1,0:T(8,128)(2,1)S(1)} %convolution_convert_fusion.1.v_ref, ...), custom_call_target="tpu_custom_call" | custom-call | flops 4000000000 | bytes 4000000 | tf_op jit(solution)/shard_map/pallas_call | solution.py:163
  73.0 0.8 copy-done.2
  73.8 0.6 copy-done.5
  74.4 1.0 copy-done.17
  75.3 0.8 copy-done.21
  76.1 2.5 %all-gather.6.cloned.1.call-done = bf16[2048,2048]{1,0:T(8,128)(2,1)} async-done(((bf16[512,2048]{1,0:T(8,128)(2,1)}), bf16[2048,2048]{1,0:T(8,128)(2,1)}) %all-gather.6.cloned.1.call-update) | async-done | bytes 8388624 | tf_op jit(solution)/shard_map/all_gather | solution.py:447
  78.7 0.0 all-gather.8.cloned.1.call-update
  78.7 1.2 convolution_convert_fusion.6
  79.9 0.1 copy.32
  80.0 1.5 convolution_convert_fusion.4
  81.6 0.5 convolution_convert_fusion.3
  82.0 0.0 copy-start.8
  82.1 31.0 %all_gather.23 = bf16[512,800]{1,0:T(8,128)(2,1)S(1)} all-gather(bf16[128,800]{1,0:T(8,128)(2,1)S(1)} %pad_maximum_fusion.2), channel_id=1, replica_groups=mesh['grp'=2,'sp'=4,'tp'=4] {'sp'}, dimensions={0}, use_global_device_ids=true | all-gather | bytes 1024000 | tf_op jit(solution)/shard_map/all_gather | solution.py:460
  113.2 0.0 copy-start.30
  113.2 6.1 %shard_map.174.start_ref = f32[2,256,512]{2,1,0:T(8,128)S(1)} custom-call(bf16[512,256]{1,0:T(8,128)(2,1)S(1)} %slice.26.k_ref, bf16[512,512]{1,0:T(8,128)(2,1)S(1)} %slice.27.v_ref, bf16[512,32]{1,0:T(8,128)(2,1)S(1)} %slice.28.low_ref, bf16[2,16,256]{2,1,0:T(8,128)(2,1)S(1)} %constant_dynamic-slice_fusion.1.dw_ref, f32[2,256]{1,0:T(2,128)S(1)} %copy-done.8), custom_call_target="tpu_custom_call" | custom-call | flops 4000000000 | bytes 4000000 | tf_op jit(solution)/shard_map/pallas_call | solution.py:163
  119.3 0.0 copy-done.24
  119.3 0.0 copy-done.30
  119.3 0.0 copy-start.19
  119.3 0.0 copy-start.6
  119.3 0.0 copy-start.15
  119.3 2.0 %convolution_convert_fusion.gate_ref = bf16[512,512]{1,0:T(8,128)(2,1)} fusion(bf16[512,2048]{1,0:T(8,128)(2,1)S(1)} %copy-done.24, bf16[2048,512]{1,0:T(8,128)(2,1)S(1)} %copy-done.30), kind=kOutput, calls=%fused_computation.2 | convolution fusion | flops 1074003968 | bytes 4718592 | tf_op jit(solution)/shard_map/dot_general | solution.py:415
  121.3 0.0 copy-done.19
  121.3 12.7 %all-gather.2.totals_ref = f32[4,2,256]{2,1,0:T(2,128)S(1)} all-gather(f32[1,2,256]{2,1,0:T(2,128)S(1)} %bitcast.32), channel_id=3, replica_groups=mesh['grp'=2,'sp'=4,'tp'=4] {'sp'}, dimensions={0}, use_global_device_ids=true | all-gather | bytes 10240 | tf_op jit(solution)/shard_map/all_gather | solution.py:494
  134.0 1.4 all-gather.8.cloned.1.call-done
  135.5 1.6 copy-done.9
  137.1 1.0 copy-done.16
  138.1 1.2 copy-done.18
  139.3 1.2 copy-done.20
  140.6 1.0 copy-done.22
  141.6 1.6 shard_map.175
  143.2 0.0 copy-start.4
  143.2 1.0 copy.33
  144.2 12.3 %all_to_all.19 = bf16[4,128,512]{1,2,0:T(8,128)(2,1)S(1)} all-to-all(bf16[4,128,512]{1,2,0:T(8,128)(2,1)} %copy.33), channel_id=1, replica_groups=mesh['grp'=2,'sp'=4,'tp'=4] {'tp'}, dimensions={0} | all-to-all | bytes 1048576 | tf_op jit(solution)/shard_map/all_to_all | solution.py:512
  156.5 4.8 %fusion.10 = (f32[128]{0:T(128)S(1)}, f32[128,2048]{1,0:T(8,128)S(1)}) fusion(bf16[128,2048]{0,1:T(8,128)(2,1)S(1)} %bitcast.36, bf16[2048,2048]{1,0:T(8,128)(2,1)} %all-gather.6.cloned.1.call-done, f32[2048]{0:T(1024)S(1)} %bitcast.31, bf16[128,2048]{1,0:T(8,128)(2,1)S(1)} %copy-done.1), kind=kOutput, calls=%fused_computation.41 | convolution fusion | flops 1075052416 | bytes 10494464 | tf_op jit(solution)/shard_map/dot_general | solution.py:513
  161.3 0.3 multiply_reduce_fusion
  161.6 1.0 add_convert_fusion
  (44 shorter events, 0.2 us)
Async XLA Ops:
  6.5 59.5 %copy-start = (bf16[2048,512]{1,0:T(8,128)(2,1)S(1)}, bf16[2048,512]{1,0:T(8,128)(2,1)}, u32[]{:S(2)}) copy-start(bf16[2048,512]{1,0:T(8,128)(2,1)} %param.26) | copy-start | bytes 6291460
  6.5 1.7 %copy-start.28 = (f32[512]{0:T(512)S(1)}, f32[512]{0:T(512)}, u32[]{:S(2)}) copy-start(f32[512]{0:T(512)} %param.21) | copy-start | bytes 6148
  6.5 1.7 %copy-start.29 = (f32[512]{0:T(512)S(1)}, f32[512]{0:T(512)}, u32[]{:S(2)}) copy-start(f32[512]{0:T(512)} %param.20) | copy-start | bytes 6148
  6.5 1.7 %copy-start.1 = (bf16[128,2048]{1,0:T(8,128)(2,1)S(1)}, bf16[128,2048]{1,0:T(8,128)(2,1)}, u32[]{:S(2)}) copy-start(bf16[128,2048]{1,0:T(8,128)(2,1)} %latent_ref.1) | copy-start | bytes 1572868
  6.5 1.8 %copy-start.14 = (f32[6144]{0:T(1024)S(1)}, f32[6144]{0:T(1024)}, u32[]{:S(2)}) copy-start(f32[6144]{0:T(1024)} %param.23) | copy-start | bytes 73732
  6.5 72.1 %all-gather.6.cloned.1.call-start = ((), (), s32[]{:S(2)}) async-start(), calls=%async_computation.1 | async-start | bytes 10485760 | tf_op jit(solution)/shard_map/all_gather | solution.py:447
  7.3 128.2 %all-gather.8.cloned.1.call-start = ((), (), s32[]{:S(2)}) async-start(), calls=%async_computation.2 | async-start | bytes 2621440 | tf_op jit(solution)/shard_map/all_gather | solution.py:493
  8.3 1.4 copy-start.10
  9.7 1.2 copy-start.11
  10.9 1.2 copy-start.12
  12.2 1.0 copy-start.13
  13.2 43.8 %copy-start.25 = (bf16[2048,32]{0,1:T(8,128)(2,1)S(1)}, bf16[2048,32]{0,1:T(8,128)(2,1)}, u32[]{:S(2)}) copy-start(bf16[2048,32]{0,1:T(8,128)(2,1)} %param.28) | copy-start | bytes 393220
  56.4 0.6 copy-start.3
  61.6 5.8 %copy-start.7 = (f32[2,256]{1,0:T(2,128)}, f32[2,256]{1,0:T(2,128)S(1)}, u32[]{:S(2)}) copy-start(f32[2,256]{1,0:T(2,128)S(1)} %constant_dynamic-slice_fusion.db_ref) | copy-start | bytes 6148
  62.3 2.5 %copy-start.23 = (bf16[512,2048]{1,0:T(8,128)(2,1)S(1)}, bf16[512,2048]{1,0:T(8,128)(2,1)}, u32[]{:S(2)}) copy-start(bf16[512,2048]{1,0:T(8,128)(2,1)} %get-tuple-element.17) | copy-start | bytes 6291460
  62.3 2.5 %copy-start.31 = (bf16[2048,512]{1,0:T(8,128)(2,1)S(1)}, bf16[2048,512]{1,0:T(8,128)(2,1)}, u32[]{:S(2)}) copy-start(bf16[2048,512]{1,0:T(8,128)(2,1)} %get-tuple-element.18) | copy-start | bytes 6291460
  72.9 0.8 copy-start.2
  73.8 0.6 copy-start.5
  74.4 1.0 copy-start.17
  75.3 0.8 copy-start.21
  82.0 31.1 %copy-start.8 = (f32[2,256]{1,0:T(2,128)S(1)}, f32[2,256]{1,0:T(2,128)}, u32[]{:S(2)}) copy-start(f32[2,256]{1,0:T(2,128)} %copy-done.7) | copy-start | bytes 6148
  113.2 6.1 %copy-start.24 = (bf16[512,2048]{1,0:T(8,128)(2,1)S(1)}, bf16[512,2048]{1,0:T(8,128)(2,1)}, u32[]{:S(2)}) copy-start(bf16[512,2048]{1,0:T(8,128)(2,1)} %get-tuple-element.17) | copy-start | bytes 6291460
  113.2 6.1 %copy-start.30 = (bf16[2048,512]{1,0:T(8,128)(2,1)S(1)}, bf16[2048,512]{1,0:T(8,128)(2,1)}, u32[]{:S(2)}) copy-start(bf16[2048,512]{1,0:T(8,128)(2,1)} %param.27) | copy-start | bytes 6291460
  119.3 2.1 %copy-start.19 = (f32[2,256,512]{2,1,0:T(8,128)}, f32[2,256,512]{2,1,0:T(8,128)S(1)}, u32[]{:S(2)}) copy-start(f32[2,256,512]{2,1,0:T(8,128)S(1)} %shard_map.174.start_ref) | copy-start | bytes 3145732
  119.3 2.1 %copy-start.6 = (f32[2,256]{1,0:T(2,128)S(1)}, f32[2,256]{1,0:T(2,128)}, u32[]{:S(2)}) copy-start(f32[2,256]{1,0:T(2,128)} %copy-done.5) | copy-start | bytes 6148
  119.3 16.2 %copy-start.15 = (f32[512]{0:T(512)S(1)}, f32[512]{0:T(512)}, u32[]{:S(2)}) copy-start(f32[512]{0:T(512)} %param.32) | copy-start | bytes 6148
  135.5 1.6 copy-start.9
  137.1 1.0 copy-start.16
  138.1 1.2 copy-start.18
  139.3 1.2 copy-start.20
  140.6 1.0 copy-start.22
  143.2 13.3 %copy-start.4 = (f32[1,2048]{1,0:T(1,128)S(1)}, f32[1,2048]{1,0:T(1,128)}, u32[]{:S(2)}) copy-start(f32[1,2048]{1,0:T(1,128)} %copy-done.3) | copy-start | bytes 24580
  156.5 5.1 %copy-start.26 = (f32[2048]{0:T(1024)S(1)}, f32[2048]{0:T(1024)}, u32[]{:S(2)}) copy-start(f32[2048]{0:T(1024)} %param.35) | copy-start | bytes 24580
  156.5 5.1 %copy-start.27 = (f32[2048]{0:T(1024)S(1)}, f32[2048]{0:T(1024)}, u32[]{:S(2)}) copy-start(f32[2048]{0:T(1024)} %param.34) | copy-start | bytes 24580
Sparse Core Ops, SparseCore 0:
  8.9 69.7 all-gather.5
  80.2 55.1 all-gather.7
where the time goes:
time: 170 us; the launch traced here: 169 us
  Pallas kernels  56.5 us (33%)
  blocking collectives  55.9 us (33%)
  local copies, waits for them, and re-layouts  19.3 us (11%)
  matrix products  15.4 us (9%)
  between operations  13.8 us (8%)
  waiting for transfers between devices  4.67 us (3%)
  other arithmetic  3.81 us (2%)
    pallas_call x1, Pallas kernels, comm_call(): pl.pallas_call(kernel, out_shape=out_shape, in_specs=[pl.BlockSpec(memory...  43.2 us
    all_gather x1, blocking collectives, body(): gathered_context = lax.all_gather(context_local, 'sp', axis=0, tiled=True)  31 us
    unnamed x64, local copies, waits for them, and re-layouts  14.8 us
    pallas_call x3, Pallas kernels, call(): pl.pallas_call(kernel, out_shape=out_shape, in_specs=[pl.BlockSpec(memory...  13.3 us
    all_gather x1, blocking collectives, body(): all_totals = lax.all_gather(totals, 'sp')  12.7 us
    all_to_all x1, blocking collectives, body(): lax.all_to_all(gated_rows, 'tp', split_axis=0, concat_axis=1, tiled=True)  12.3 us
    dot_general x7, matrix products, project(): return jnp.dot(rows, weight, preferred_element_type=f32).astype(bf16)  10.6 us
    dot_general x1, matrix products, body(): branch = jnp.dot(regrouped, full_out, preferred_element_type=f32)  4.79 us
  transfers between devices with their start and end apart: 2, of which 2 were waited for; matrix products, arithmetic and copies ran while one was open for 10% of the time, Pallas kernels for 32%

commit v1 on v0

--- a/solution.py
+++ b/solution.py
@@ -1,4 +1,5 @@
 import functools
+from typing import Any, NamedTuple
 
 import jax
 import jax.numpy as jnp
@@ -518,6 +519,638 @@
     return (centered * lax.rsqrt(variance + norm_eps) * final_gain + final_bias).astype(bf16)
 
 
+class Scratch(NamedTuple):
+    cond: Any
+    ctx_cond: Any
+    mod_w: Any
+    mod_b: Any
+    wqk: Any
+    rows: Any
+    mod_latent: Any
+    context: Any
+    mod_context: Any
+    low_w: Any
+    value_w: Any
+    gate_w: Any
+    out_w: Any
+    decay_w: Any
+    decay_b: Any
+    extra: Any
+    norm_gain: Any
+    final_gain: Any
+    final_bias: Any
+    part: Any
+    sums: Any
+    totals: Any
+    shifts: Any
+    scales: Any
+    branch_gate: Any
+    cosine: Any
+    sine: Any
+    ctx_close: Any
+    ctx_value: Any
+    low: Any
+    value: Any
+    gate: Any
+    key: Any
+    cum: Any
+    ahead: Any
+    total: Any
+    start: Any
+    state: Any
+    carry: Any
+    own_decay: Any
+    ahead_decay: Any
+    chain_in: Any
+    chain_out: Any
+    q_all: Any
+    mixture: Any
+    joined: Any
+    gated: Any
+    pair_out: Any
+    pair_in: Any
+    far_out: Any
+    far_in: Any
+    branch: Any
+    load_sem: Any
+    zs: Any
+    zr: Any
+    ys: Any
+    yr: Any
+    xs: Any
+    xr: Any
+    cs: Any
+    cr: Any
+    ps: Any
+    pr: Any
+    ts: Any
+    tr: Any
+    ss: Any
+    sr: Any
+    hs: Any
+    hr: Any
+    ds: Any
+    dr: Any
+    fs: Any
+    fr: Any
+
+
+def spread_of(ref, axis, send_sem, recv_sem):
+    return (lambda: spread(ref, axis, send_sem, recv_sem),
+            lambda: spread_arrive(ref, axis, send_sem, recv_sem),
+            lambda: spread_drain(ref, axis, send_sem, recv_sem))
+
+
+PARTS = 2
+
+
+def fused_kernel(latent, context, cond, ctx_cond, mod_w, mod_b, query_w, key_w, value_w, gate_w,
+                 low_w, decay_w, decay_b, extra, norm_gain, out_w, final_gain, final_bias,
+                 out_ref, s):
+    grp = lax.axis_index("grp")
+    sp, sp_count = lax.axis_index("sp"), lax.axis_size("sp")
+    tp, tp_count = lax.axis_index("tp"), lax.axis_size("tp")
+    own, width = latent.shape
+    depth = query_w.shape[0]
+    keys = query_w.shape[1] // ATTENTION_HEADS
+    vals = value_w.shape[1]
+    count = own * tp_count
+    size = 2 * BLOCK
+    blocks = count // size
+    ctx = context.shape[0]
+    x, core = tp // 2, tp % 2
+    sibling, across = tp + 1 - 2 * core, 2 * (1 - x) + core
+    far_sibling = 2 * (1 - x) + 1 - core
+
+    def block_rows(j):
+        return pl.ds(pl.multiple_of(j * own, own), own)
+
+    ready = open_kernel([("sp", t) for t in others("sp")] + [("tp", t) for t in others("tp")]
+                        + [("grp", 1 - grp)])
+    head_cols = pl.ds(pl.multiple_of(tp * keys, keys), keys)
+    own_depth = pl.ds(pl.multiple_of(sp * depth, depth), depth)
+    loads = []
+    for i, (source, target) in enumerate((
+        (cond, s.cond), (ctx_cond, s.ctx_cond),
+        (mod_w, s.mod_w),
+        (key_w.at[:, head_cols], s.wqk.at[0, own_depth, :]),
+        (query_w.at[:, head_cols], s.wqk.at[1, own_depth, :]),
+        (latent, s.rows.at[block_rows(tp), :]),
+        (mod_b, s.mod_b), (context, s.context),
+        (low_w, s.low_w), (value_w, s.value_w),
+        (decay_w.at[:, :, head_cols], s.decay_w),
+        (decay_b.at[:, head_cols], s.decay_b), (extra, s.extra),
+        (gate_w, s.gate_w), (norm_gain, s.norm_gain),
+        (out_w, s.out_w), (final_gain, s.final_gain),
+        (final_bias, s.final_bias),
+    )):
+        loads.append(pltpu.make_async_copy(source, target, s.load_sem.at[i]))
+        loads[i].start()
+    (load_cond, load_ctx_cond, load_mod_w, load_key_w, load_query_w, load_latent,
+     load_mod_b, load_context, load_low_w, load_value_w, load_decay_w, load_decay_b,
+     load_extra, load_gate_w, load_norm_gain, load_out_w, load_final_gain, load_final_bias) = loads
+
+    half = depth // 2
+    step = half // PARTS
+
+    def weight_view(side):
+        def view(block, chunk):
+            start = block * depth + side * half + (chunk % PARTS) * step
+            return s.wqk.at[chunk // PARTS, pl.ds(pl.multiple_of(start, step), step), :]
+        return view
+
+    line = Line(sp, sp_count, "sp", lambda p: p, weight_view(grp), 2 * PARTS, s.zs, s.zr)
+    other_view = weight_view(1 - grp)
+
+    def y_copy(ref, way, hop, chunk):
+        return remote(ref, ref, s.ys.at[way, hop, chunk], s.yr.at[way, hop, chunk],
+                      "grp", 1 - grp)
+
+    def z_arrive(hop, chunk):
+        for way in range(2):
+            line.arrive(way, hop, chunk, lambda block: y_copy(
+                weight_view(grp)(block, chunk), way, hop, chunk).start())
+            if hop + 1 < sp_count - 1:
+                line.send(way, hop + 1, chunk)
+
+    def y_each(hop, chunk, view, act):
+        for way in range(2):
+            block = sp - 1 - hop if way == 0 else sp + 1 + hop
+            valid = sp > hop if way == 0 else sp + 1 + hop < sp_count
+
+            @pl.when(valid)
+            def _():
+                act(y_copy(view(block, chunk), way, hop, chunk))
+
+    key_chunks, query_chunks = range(PARTS), range(PARTS, 2 * PARTS)
+
+    def send_own(chunks):
+        for chunk in chunks:
+            for way in range(2):
+                line.send(way, 0, chunk)
+
+    pieces = s.xs.shape[0]
+    piece = own // pieces
+
+    def rows_piece(j, p):
+        return s.rows.at[pl.ds(pl.multiple_of(j * own + p * piece, piece), piece), :]
+
+    def x_copy(j, p):
+        return remote(rows_piece(j, p), rows_piece(j, p), s.xs.at[p], s.xr.at[p],
+                      "tp", across)
+
+    def cross(j, p, slot):
+        k = slot * pieces + p
+        return remote(rows_piece(j, p), rows_piece(j, p), s.cs.at[k], s.cr.at[k],
+                      "tp", sibling)
+
+    part_go, part_arrive, part_drain = spread_of(s.part, "sp", s.ps, s.pr)
+    sums_go, sums_arrive, sums_drain = spread_of(s.sums, "tp", s.ss, s.sr)
+    tot_go, tot_arrive, tot_drain = spread_of(s.totals, "sp", s.ts, s.tr)
+
+    for load in (load_cond, load_ctx_cond, load_mod_w):
+        load.wait()
+    v = jnp.concatenate([s.cond[...], s.ctx_cond[...]], axis=0)
+    activated = (v / (1.0 + jnp.exp(-v))).astype(bf16)
+    s.part[sp] = dot(activated, s.mod_w[...])
+    for load in (load_key_w, load_query_w, load_latent):
+        load.wait()
+
+    ready()
+    part_go()
+    send_own(key_chunks)
+    send_own(query_chunks[:1])
+    for p in range(pieces):
+        if p < pieces // 2:
+            x_copy(tp, p).start()
+        cross(tp, p, 0).start()
+
+    quarter = keys // 4
+
+    def rope(b, carry):
+        rows = pl.ds(pl.multiple_of(b * size, size), size)
+        lane = lax.broadcasted_iota(jnp.int32, (1, keys), 1)
+        index = jnp.bitwise_and(lane, quarter - 1).astype(f32)
+        frequency = jnp.exp(index * (-jnp.log(rope_base) / quarter))
+        by_row = lane < keys // 2
+        first = jnp.bitwise_and(lane, 2 * quarter - 1) < quarter
+        place = lax.broadcasted_iota(jnp.int32, (size, 1), 0) + (sp * count + b * size)
+        place = place.astype(f32)
+        row = jnp.floor((place + 0.5) * (1.0 / GRID_W))
+        col = place - row * GRID_W
+        angle = jnp.where(by_row, row, col) * frequency
+        s.cosine[rows, :] = jnp.cos(angle)
+        sine = jnp.sin(angle)
+        s.sine[rows, :] = jnp.where(first, -sine, sine)
+        return carry
+
+    lax.fori_loop(0, blocks, rope, 0)
+
+    @pl.when(sp == 0)
+    def _():
+        s.chain_in[0] = jnp.zeros(s.chain_in.shape[1:], bf16)
+
+    @pl.when(sp == sp_count - 1)
+    def _():
+        s.chain_in[1] = jnp.zeros(s.chain_in.shape[1:], bf16)
+
+    part_arrive()
+    total = s.part[0]
+    for j in range(1, sp_count):
+        total = total + s.part[j]
+    s.sums[tp] = total
+    sums_go()
+    for p in range(pieces // 2, pieces):
+        x_copy(tp, p).start()
+    for chunk in key_chunks:
+        z_arrive(0, chunk)
+    send_own(query_chunks[1:])
+    sums_arrive()
+    for load in (load_mod_b, load_context, load_low_w, load_value_w, load_decay_w, load_decay_b, load_extra):
+        load.wait()
+    modulation = (jnp.concatenate([s.sums[j] for j in range(tp_count)], axis=1)
+                  + s.mod_b[...])
+    s.shifts[...] = modulation[:, :width]
+    s.scales[...] = 1.0 + modulation[:, width:2 * width]
+    s.branch_gate[...] = modulation[0:1, 2 * width:]
+    s.mod_context[...] = (s.context[...].astype(f32) * s.scales[1:2, :]
+                             + s.shifts[1:2, :]).astype(bf16)
+
+    def decay_of(low, direction):
+        rank = s.decay_w.shape[1]
+        logits = dot(low[:, direction * rank:(direction + 1) * rank], s.decay_w[direction])
+        return log_sigmoid(logits + s.decay_b[direction:direction + 1, :]) / gate_scale
+
+    ctx_low = dot(s.mod_context[...], s.low_w[...], ((1,), (1,))).astype(bf16)
+    ctx_totals = []
+    for direction in range(2):
+        mask = triangle(ctx, direction == 1).astype(f32)
+        edge = 0 if direction == 1 else ctx - 1
+        cum = dot(mask, decay_of(ctx_low, direction), precision=highest)
+        ctx_totals.append(cum[edge:edge + 1, :])
+        s.ctx_close[direction] = jnp.exp(ctx_totals[direction] - cum)
+    s.ctx_value[...] = dot(s.mod_context[...], s.value_w[...]).astype(bf16)
+    load_gate_w.wait()
+
+    def project_chip(chip):
+        rows = pl.ds(pl.multiple_of(chip * 2 * own, 2 * own), 2 * own)
+        mod = (s.rows[rows, :].astype(f32) * s.scales[0:1, :]
+               + s.shifts[0:1, :]).astype(bf16)
+        s.mod_latent[rows, :] = mod
+        s.low[rows, :] = dot(mod, s.low_w[...], ((1,), (1,))).astype(bf16)
+        s.value[rows, :] = dot(mod, s.value_w[...]).astype(bf16)
+        s.gate[rows, :] = dot(mod, s.gate_w[...]).astype(bf16)
+
+    for chunk in key_chunks:
+        if sp_count > 2:
+            z_arrive(1, chunk)
+    for p in range(pieces):
+        cross(tp, p, 0).wait_send()
+        remote(rows_piece(sibling, p), rows_piece(sibling, p), s.cs.at[p], s.cr.at[p],
+               "tp", sibling).wait_recv()
+    project_chip(x)
+    for chunk in query_chunks:
+        z_arrive(0, chunk)
+    for p in range(pieces):
+        x_copy(across, p).wait_recv()
+        cross(across, p, 1).start()
+    for hop in range(2, sp_count - 1):
+        for chunk in key_chunks:
+            z_arrive(hop, chunk)
+    for p in range(pieces):
+        cross(far_sibling, p, 1).wait_recv()
+    project_chip(1 - x)
+
+    own_head = lax.broadcasted_iota(jnp.int32, (ATTENTION_HEADS, size), 0) == tp
+    for direction in range(2):
+        mask = triangle(size, direction == 1).astype(f32)
+        edge = 0 if direction == 1 else size - 1
+        before = None
+        for turn in range(blocks):
+            b = blocks - 1 - turn if direction == 1 else turn
+            rows = slice(b * size, (b + 1) * size)
+            head_extra = jnp.sum(jnp.where(own_head, s.extra[direction, :, rows], 0.0), axis=0,
+                                 keepdims=True)
+            added = jnp.sum(mask * head_extra, axis=1, keepdims=True)
+            cum = dot(mask, decay_of(s.low[rows, :], direction), precision=highest) + added
+            s.cum[direction, rows, :] = cum
+            block_total = cum[edge:edge + 1, :]
+            if before is not None:
+                s.ahead[direction, b:b + 1, :] = before
+            before = block_total if before is None else before + block_total
+        s.total[direction:direction + 1, :] = before
+    s.totals[sp] = jnp.concatenate([s.total[...]] + ctx_totals, axis=0)
+    tot_go()
+
+    for hop in range(sp_count - 1):
+        for chunk in key_chunks:
+            y_each(hop, chunk, other_view, lambda c: c.wait_recv())
+    ctx_key = dot(s.mod_context[...], s.wqk[0]).astype(bf16).astype(f32)
+    for direction in range(2):
+        closing = (ctx_key * s.ctx_close[direction]).astype(bf16)
+        s.carry[direction] = dot(closing, s.ctx_value[...], ((0,), (0,)))
+    for b in range(blocks):
+        rows = slice(b * size, (b + 1) * size)
+        key = dot(s.mod_latent[rows, :], s.wqk[0]).astype(bf16)
+        s.key[rows, :] = rotate(key.astype(f32), s.cosine[rows, :], s.sine[rows, :])
+    if sp_count > 2:
+        for chunk in query_chunks:
+            z_arrive(1, chunk)
+    for direction in range(2):
+        edge = 0 if direction == 1 else size - 1
+        state = None
+        for turn in range(blocks):
+            b = blocks - 1 - turn if direction == 1 else turn
+            rows = slice(b * size, (b + 1) * size)
+            cum = s.cum[direction, rows, :]
+            block_total = cum[edge:edge + 1, :]
+            closing = (s.key[rows, :] * jnp.exp(block_total - cum)).astype(bf16)
+            term = dot(closing, s.value[rows, :], ((0,), (0,)))
+            if state is None:
+                state = term
+            else:
+                s.start[direction, b] = state.astype(bf16)
+                state = jnp.exp(block_total).T * state + term
+        s.state[direction] = state
+    tot_arrive()
+    chunk_width = s.chain_in.shape[3]
+    chunk_count = s.chain_in.shape[1]
+
+    def column(row):
+        return jnp.broadcast_to(jnp.exp(row).T, (keys, chunk_width))
+
+    for direction in range(2):
+        ahead = jnp.zeros((1, keys), f32)
+        after = jnp.zeros((1, keys), f32)
+        for j in range(sp_count):
+            upstream = (j > sp) if direction == 1 else (j < sp)
+            downstream = (j < sp) if direction == 1 else (j > sp)
+            ahead = ahead + jnp.where(upstream, s.totals[j, direction:direction + 1, :], 0.0)
+            after = after + jnp.where(
+                downstream, s.totals[j, 2 + direction:3 + direction, :], 0.0)
+        s.own_decay[direction] = column(s.total[direction:direction + 1, :])
+        s.ahead_decay[direction] = column(ahead)
+        after_decay = column(after)
+        for c in range(chunk_count):
+            cols = slice(c * chunk_width, (c + 1) * chunk_width)
+            carried = after_decay * s.carry[direction, :, cols]
+            s.carry[direction, :, cols] = carried
+            s.state[direction, :, cols] += (
+                s.own_decay[direction] * s.ahead_decay[direction] * carried)
+
+    first_way = jnp.where(sp < sp_count // 2, 0, 1)
+
+    def chain_copy(way, c, target):
+        return remote(s.chain_out.at[way, c], s.chain_in.at[way, c], s.hs.at[way, c],
+                      s.hr.at[way, c], "sp", target)
+
+    def chain(way, c, sources):
+        cols = slice(c * chunk_width, (c + 1) * chunk_width)
+        onward = 1 - 2 * way
+        has_before = jnp.where(way == 0, sp > 0, sp < sp_count - 1)
+        has_next = jnp.where(way == 0, sp < sp_count - 1, sp > 0)
+
+        @pl.when(jnp.logical_and(has_next, jnp.logical_not(has_before)) if sources else has_before)
+        def _():
+            if not sources:
+                chain_copy(way, c, sp - onward).wait_recv()
+
+            @pl.when(has_next)
+            def _():
+                s.chain_out[way, c, :keys, :] = (
+                    s.own_decay[way] * s.chain_in[way, c, :keys, :].astype(f32)
+                    + s.state[way, :, cols]).astype(bf16)
+                s.chain_out[way, c, keys:, :] = (
+                    s.chain_in[way, c, keys:, :].astype(f32)
+                    + s.carry[1 - way, :, cols]).astype(bf16)
+                chain_copy(way, c, sp + onward).start()
+
+    def attend(b):
+        rows = slice(b * size, (b + 1) * size)
+        query = dot(s.mod_latent[rows, :], s.wqk[1]).astype(bf16)
+        rq = rotate(query.astype(f32) * keys ** -0.5, s.cosine[rows, :], s.sine[rows, :])
+        rk = s.key[rows, :]
+        scores, out = None, None
+        for direction in range(2):
+            keep = triangle(size, direction == 1)
+            middle = size // 2 if direction == 1 else size // 2 - 1
+            cum = s.cum[direction, rows, :]
+            center = cum[middle:middle + 1, :]
+            q_mid = (rq * jnp.exp(cum - center)).astype(bf16)
+            k_mid = (rk * jnp.exp(center - cum)).astype(bf16)
+            score = jnp.where(keep, dot(q_mid, k_mid, ((1,), (1,))), 0.0)
+            scores = score if scores is None else scores + score
+            q_dec = rq * jnp.exp(cum)
+            q_all = q_dec
+            if b != (blocks - 1 if direction == 1 else 0):
+                carried = dot(q_dec.astype(bf16), s.start[direction, b])
+                out = carried if out is None else out + carried
+                q_all = q_dec * jnp.exp(s.ahead[direction, b:b + 1, :])
+            s.q_all[rows, direction * keys:(direction + 1) * keys] = q_all.astype(bf16)
+        inner = dot(scores.astype(bf16), s.value[rows, :])
+        s.mixture[rows, :] = inner if out is None else out + inner
+
+    for c in range(chunk_count):
+        chain(first_way, c, True)
+    for hop in range(2, sp_count - 1):
+        for chunk in query_chunks:
+            z_arrive(hop, chunk)
+    for hop in range(sp_count - 1):
+        for chunk in query_chunks:
+            y_each(hop, chunk, other_view, lambda c: c.wait_recv())
+    for turn in range(max(blocks, chunk_count)):
+        if turn < blocks:
+            attend(turn)
+        if turn < chunk_count:
+            chain(first_way, turn, False)
+    for c in range(chunk_count):
+        chain(1 - first_way, c, False)
+    for c in range(chunk_count):
+        cols = slice(c * chunk_width, (c + 1) * chunk_width)
+        for direction in range(2):
+            joined = (s.chain_in[direction, c, :keys, :].astype(f32)
+                      + s.ahead_decay[direction]
+                      * (s.carry[direction, :, cols]
+                         + s.chain_in[1 - direction, c, keys:, :].astype(f32)))
+            s.joined[direction * keys:(direction + 1) * keys, cols] = joined.astype(bf16)
+    for load in (load_norm_gain, load_out_w, load_final_gain, load_final_bias):
+        load.wait()
+
+    def gate_rows(chip):
+        rows = pl.ds(pl.multiple_of(chip * 2 * own, 2 * own), 2 * own)
+        mixture = s.mixture[rows, :] + dot(s.q_all[rows, :], s.joined[...])
+        squares = jnp.mean(mixture * mixture, axis=1, keepdims=True)
+        gate = s.gate[rows, :].astype(f32)
+        normed = mixture * lax.rsqrt(squares + norm_eps) * s.norm_gain[...]
+        s.gated[rows, :] = (normed * (gate / (1.0 + jnp.exp(-gate)))).astype(bf16)
+
+    out_chunks = s.far_out.shape[0]
+    out_width = width // out_chunks
+
+    def product(j, n):
+        cols = slice(n * out_width, (n + 1) * out_width)
+        return dot(s.gated[block_rows(j), :], s.out_w[:, cols])
+
+    def pair_copy(slot, n):
+        return remote(s.pair_out.at[slot, n], s.pair_in.at[slot, n], s.ds.at[slot, n],
+                      s.dr.at[slot, n], "tp", sibling)
+
+    def far_copy(n):
+        return remote(s.far_out.at[n], s.far_in.at[n], s.fs.at[n], s.fr.at[n],
+                      "tp", across)
+
+    gate_rows(1 - x)
+    for n in range(out_chunks):
+        s.pair_out[0, n] = product(far_sibling, n).astype(bf16)
+        pair_copy(0, n).start()
+    for n in range(out_chunks):
+        mine = product(across, n)
+        pair_copy(0, n).wait_recv()
+        s.far_out[n] = (mine + s.pair_in[0, n].astype(f32)).astype(bf16)
+        far_copy(n).start()
+    gate_rows(x)
+    for n in range(out_chunks):
+        s.pair_out[1, n] = product(sibling, n).astype(bf16)
+        pair_copy(1, n).start()
+    for n in range(out_chunks):
+        cols = slice(n * out_width, (n + 1) * out_width)
+        mine = product(tp, n)
+        pair_copy(1, n).wait_recv()
+        s.branch[:, cols] = mine + s.pair_in[1, n].astype(f32)
+    for n in range(out_chunks):
+        cols = slice(n * out_width, (n + 1) * out_width)
+        far_copy(n).wait_recv()
+        branch = s.branch[:, cols] + s.far_in[n].astype(f32)
+        s.branch[:, cols] = (residual_scale * s.rows[block_rows(tp), cols].astype(f32)
+                                + s.branch_gate[:, cols] * branch)
+    summed = s.branch[...]
+    centered = summed - jnp.mean(summed, axis=1, keepdims=True)
+    variance = jnp.mean(centered * centered, axis=1, keepdims=True)
+    out_ref[...] = (centered * lax.rsqrt(variance + norm_eps) * s.final_gain[...]
+                    + s.final_bias[...]).astype(bf16)
+
+    part_drain()
+    sums_drain()
+    tot_drain()
+    line.drain()
+    for hop in range(sp_count - 1):
+        for chunk in range(2 * PARTS):
+            y_each(hop, chunk, weight_view(grp), lambda c: c.wait_send())
+    for p in range(pieces):
+        x_copy(tp, p).wait_send()
+        cross(across, p, 1).wait_send()
+    for way in range(2):
+        has_next = sp < sp_count - 1 if way == 0 else sp > 0
+
+        @pl.when(has_next)
+        def _():
+            for c in range(chunk_count):
+                chain_copy(way, c, sp + 1 if way == 0 else sp - 1).wait_send()
+    for n in range(out_chunks):
+        pair_copy(0, n).wait_send()
+        pair_copy(1, n).wait_send()
+        far_copy(n).wait_send()
+
+
+def fused(latent, context, condition, context_condition, mod_weight, mod_bias, query_weight,
+          key_weight, value_weight, out_gate_weight, decay_in_weight, decay_weight, decay_bias,
+          extra_decay, norm_gain, out_weight, final_gain, final_bias):
+    sp_count, tp_count = lax.axis_size("sp"), lax.axis_size("tp")
+    own, width = latent.shape
+    depth = query_weight.shape[0]
+    keys = query_weight.shape[1] // ATTENTION_HEADS
+    vals = value_weight.shape[1]
+    ctx = context.shape[0]
+    count = own * tp_count
+    blocks = count // (2 * BLOCK)
+    mod_cols = mod_weight.shape[1]
+    chains, outs, pieces = 4, 4, 4
+    args = (latent, context, condition[None, :], context_condition[None, :], mod_weight,
+            mod_bias[None, :], query_weight, key_weight, value_weight, out_gate_weight,
+            decay_in_weight.T, decay_weight, decay_bias, extra_decay, norm_gain[None, :],
+            out_weight, final_gain[None, :], final_bias[None, :])
+    dma, vmem = pltpu.SemaphoreType.DMA, pltpu.VMEM
+    hops = sp_count - 1
+    scratch = Scratch(
+        cond=vmem((1, condition.shape[0]), f32),
+        ctx_cond=vmem((1, condition.shape[0]), f32),
+        mod_w=vmem(mod_weight.shape, bf16),
+        mod_b=vmem((1, mod_bias.shape[0]), f32),
+        wqk=vmem((2, depth * sp_count, keys), bf16),
+        rows=vmem((count, width), bf16),
+        mod_latent=vmem((count, width), bf16),
+        context=vmem(context.shape, bf16),
+        mod_context=vmem(context.shape, bf16),
+        low_w=vmem(decay_in_weight.shape[::-1], bf16),
+        value_w=vmem(value_weight.shape, bf16),
+        gate_w=vmem(out_gate_weight.shape, bf16),
+        out_w=vmem(out_weight.shape, bf16),
+        decay_w=vmem(decay_weight.shape[:2] + (keys,), bf16),
+        decay_b=vmem((2, keys), f32),
+        extra=vmem(extra_decay.shape, f32),
+        norm_gain=vmem((1, vals), f32),
+        final_gain=vmem((1, width), f32),
+        final_bias=vmem((1, width), f32),
+        part=vmem((sp_count, 2, mod_cols), f32),
+        sums=vmem((tp_count, 2, mod_cols), f32),
+        totals=vmem((sp_count, 4, keys), f32),
+        shifts=vmem((2, width), f32),
+        scales=vmem((2, width), f32),
+        branch_gate=vmem((1, width), f32),
+        cosine=vmem((count, keys), f32),
+        sine=vmem((count, keys), f32),
+        ctx_close=vmem((2, ctx, keys), f32),
+        ctx_value=vmem((ctx, vals), bf16),
+        low=vmem((count, decay_in_weight.shape[1]), bf16),
+        value=vmem((count, vals), bf16),
+        gate=vmem((count, vals), bf16),
+        key=vmem((count, keys), f32),
+        cum=vmem((2, count, keys), f32),
+        ahead=vmem((2, blocks, keys), f32),
+        total=vmem((2, keys), f32),
+        start=vmem((2, blocks, keys, vals), bf16),
+        state=vmem((2, keys, vals), f32),
+        carry=vmem((2, keys, vals), f32),
+        own_decay=vmem((2, keys, vals // chains), f32),
+        ahead_decay=vmem((2, keys, vals // chains), f32),
+        chain_in=vmem((2, chains, 2 * keys, vals // chains), bf16),
+        chain_out=vmem((2, chains, 2 * keys, vals // chains), bf16),
+        q_all=vmem((count, 2 * keys), bf16),
+        mixture=vmem((count, vals), f32),
+        joined=vmem((2 * keys, vals), bf16),
+        gated=vmem((count, vals), bf16),
+        pair_out=vmem((2, outs, own, width // outs), bf16),
+        pair_in=vmem((2, outs, own, width // outs), bf16),
+        far_out=vmem((outs, own, width // outs), bf16),
+        far_in=vmem((outs, own, width // outs), bf16),
+        branch=vmem((own, width), f32),
+        load_sem=dma((len(args),)),
+        zs=dma((2, hops, 2 * PARTS)), zr=dma((2, hops, 2 * PARTS)),
+        ys=dma((2, hops, 2 * PARTS)), yr=dma((2, hops, 2 * PARTS)),
+        xs=dma((pieces,)), xr=dma((pieces,)),
+        cs=dma((2 * pieces,)), cr=dma((2 * pieces,)),
+        ps=dma((hops,)), pr=dma((hops,)), ts=dma((hops,)), tr=dma((hops,)),
+        ss=dma((tp_count - 1,)), sr=dma((tp_count - 1,)),
+        hs=dma((2, chains)), hr=dma((2, chains)),
+        ds=dma((2, outs)), dr=dma((2, outs)), fs=dma((outs,)), fr=dma((outs,)),
+    )
+    return pl.pallas_call(
+        fused_kernel,
+        out_shape=jax.ShapeDtypeStruct((own, width), bf16),
+        in_specs=[pl.BlockSpec(memory_space=pltpu.HBM)] * len(args),
+        out_specs=pl.BlockSpec(memory_space=pltpu.VMEM),
+        scratch_shapes=[scratch],
+        compiler_params=pltpu.CompilerParams(
+            vmem_limit_bytes=60 * 1024 * 1024, collective_id=2, has_side_effects=True),
+        cost_estimate=pl.CostEstimate(flops=6_000_000_000, bytes_accessed=12_000_000,
+                                      transcendentals=2_000_000),
+    )(*args)
+
+
+def whole_heads(mesh):
+    return mesh.shape["tp"] == ATTENTION_HEADS and mesh.shape["grp"] == 2
+
+
 def solution(mesh):
     placed = (
         P(("grp", "sp", "tp"), None),
@@ -540,5 +1173,5 @@
         P(),
     )
     return jax.shard_map(
-        body, mesh=mesh, in_specs=placed, out_specs=P(("grp", "sp", "tp"), None), check_vma=False
+        fused if whole_heads(mesh) else body, mesh=mesh, in_specs=placed, out_specs=P(("grp", "sp", "tp"), None), check_vma=False
     )

time: 170 us -> 75.5 us (0.44)
  blocking collectives: 55.9 us -> 0 us
  local copies, waits for them, and re-layouts: 19.3 us -> 1.88 us
  Pallas kernels: 56.5 us -> 73.4 us
  matrix products: 15.4 us -> 0 us
  between operations: 13.8 us -> 0.01 us
  waiting for transfers between devices: 4.67 us -> 0 us
  other arithmetic: 3.81 us -> 0 us
    all_gather x2 -> x0, blocking collectives: 43.7 us -> none  [the longest x1 31 us: body(): gathered_context = lax.all_gather(context_local, 'sp', axis=0, tiled=True)]
    pallas_call x4 -> x1, Pallas kernels: 56.5 us -> 73.4 us  [fused(): pl.pallas_call(fused_kernel, out_shape=jax.ShapeDtypeStruct((own, width),...]
    dot_general x8 -> x0, matrix products: 15.4 us -> none  [the longest x7 10.6 us: project(): return jnp.dot(rows, weight, preferred_element_type=f32).astype(bf16)]
    unnamed x64 -> x1, local copies, waits for them, and re-layouts: 14.8 us -> 1.88 us
    all_to_all x1 -> x0, blocking collectives: 12.3 us -> none  [body(): lax.all_to_all(gated_rows, 'tp', split_axis=0, concat_axis=1, tiled=True)]
    all_gather x2 -> x0, waiting for transfers between devices: 3.98 us -> none  [the longest x1 2.54 us: body(): full_out = lax.all_gather(out_weight, 'tp', axis=0, tiled=True)]
    dynamic_slice x4 -> x0, local copies, waits for them, and re-layouts: 2.32 us -> none  [the longest x2 0.9 us: body(): lax.dynamic_index_in_dim(extra_decay, head_index, 1, keepdims=False)]
    neg x1 -> x0, other arithmetic: 1.9 us -> none  [rope_tables(): sine = jnp.concatenate([-row_sine, row_sine, -col_sine, col_sine], axis=1)]
  transfers between devices with their start and end apart: 2 -> 0, of which waited for: 2 -> 0; matrix products, arithmetic and copies ran while one was open for 10% -> 0% of each run, Pallas kernels for 32% -> 0%
where the time goes in v1:
time: 75.5 us; the launch traced here: 75.3 us
  Pallas kernels  73.4 us (97%)
  local copies, waits for them, and re-layouts  1.88 us (2%)
    pallas_call x1, Pallas kernels, fused(): pl.pallas_call(fused_kernel, out_shape=jax.ShapeDtypeStruct((own, width),...  73.4 us
    unnamed x1, local copies, waits for them, and re-layouts  1.88 us

profile of v1, /device:TPU:0, one launch (start us, length us, event | category | flops | bytes accessed | tf_op | source)
XLA Modules:
  0.0 75.3 jit_solution(8483545763350585733)
XLA Ops:
  0.0 73.4 %shard_map.172 = bf16[128,2048]{1,0:T(8,128)(2,1)} custom-call(bf16[128,2048]{1,0:T(8,128)(2,1)} %latent.1, bf16[128,2048]{1,0:T(8,128)(2,1)} %context.1, f32[1,512]{1,0:T(1,128)} %bitcast.11, f32[1,512]{1,0:T(1,128)} %bitcast.12, bf16[512,1536]{1,0:T(8,128)(2,1)} %mod_w.1, f32[1,6144]{1,0:T(1,128)} %bitcast.8, bf16[512,1024]{1,0:T(8,128)(2,1)} %query_w.1, ...), custom_call_target="tpu_custom_call" | custom-call | flops 6000000000 | bytes 12000000 | tf_op jit(solution)/shard_map/pallas_call | solution.py:1137
  73.5 1.9 %copy.20 = bf16[128,2048]{1,0:T(8,128)(2,1)} copy(bf16[128,2048]{1,0:T(8,128)(2,1)} %shard_map.172) | data formatting | bytes 1048576

commit v2 on v1

--- a/solution.py
+++ b/solution.py
@@ -555,6 +555,7 @@
     key: Any
     cum: Any
     ahead: Any
+    block_total: Any
     total: Any
     start: Any
     state: Any
@@ -666,10 +667,10 @@
         return remote(ref, ref, s.ys.at[way, hop, chunk], s.yr.at[way, hop, chunk],
                       "grp", 1 - grp)
 
-    def z_arrive(hop, chunk):
+    def z_arrive(hop, chunk, pass_on=True):
         for way in range(2):
-            line.arrive(way, hop, chunk, lambda block: y_copy(
-                weight_view(grp)(block, chunk), way, hop, chunk).start())
+            line.arrive(way, hop, chunk, (lambda block: y_copy(
+                weight_view(grp)(block, chunk), way, hop, chunk).start()) if pass_on else None)
             if hop + 1 < sp_count - 1:
                 line.send(way, hop + 1, chunk)
 
@@ -689,7 +690,7 @@
             for way in range(2):
                 line.send(way, 0, chunk)
 
-    pieces = s.xs.shape[0]
+    pieces, early = s.xs.shape[0], 1
     piece = own // pieces
 
     def rows_piece(j, p):
@@ -721,7 +722,7 @@
     send_own(key_chunks)
     send_own(query_chunks[:1])
     for p in range(pieces):
-        if p < pieces // 2:
+        if p < early:
             x_copy(tp, p).start()
         cross(tp, p, 0).start()
 
@@ -760,7 +761,7 @@
         total = total + s.part[j]
     s.sums[tp] = total
     sums_go()
-    for p in range(pieces // 2, pieces):
+    for p in range(early, pieces):
         x_copy(tp, p).start()
     for chunk in key_chunks:
         z_arrive(0, chunk)
@@ -781,6 +782,46 @@
         logits = dot(low[:, direction * rank:(direction + 1) * rank], s.decay_w[direction])
         return log_sigmoid(logits + s.decay_b[direction:direction + 1, :]) / gate_scale
 
+    own_head = lax.broadcasted_iota(jnp.int32, (ATTENTION_HEADS, size), 0) == tp
+
+    def project_chip(chip):
+        rows = pl.ds(pl.multiple_of(chip * 2 * own, 2 * own), 2 * own)
+        mod = (s.rows[rows, :].astype(f32) * s.scales[0:1, :]
+               + s.shifts[0:1, :]).astype(bf16)
+        s.mod_latent[rows, :] = mod
+        s.low[rows, :] = dot(mod, s.low_w[...], ((1,), (1,))).astype(bf16)
+        s.value[rows, :] = dot(mod, s.value_w[...]).astype(bf16)
+
+    def gate_chip(chip):
+        rows = pl.ds(pl.multiple_of(chip * 2 * own, 2 * own), 2 * own)
+        s.gate[rows, :] = dot(s.mod_latent[rows, :], s.gate_w[...]).astype(bf16)
+
+    def decay_chip(chip):
+        for i in range(2 * own // size):
+            b = chip * (2 * own // size) + i
+            rows = pl.ds(pl.multiple_of(b * size, size), size)
+            low = s.low[rows, :]
+            for direction in range(2):
+                mask = triangle(size, direction == 1).astype(f32)
+                edge = 0 if direction == 1 else size - 1
+                head_extra = jnp.sum(jnp.where(own_head, s.extra[direction, :, rows], 0.0),
+                                     axis=0, keepdims=True)
+                added = jnp.sum(mask * head_extra, axis=1, keepdims=True)
+                cum = dot(mask, decay_of(low, direction), precision=highest) + added
+                s.cum[direction, rows, :] = cum
+                s.block_total[direction, b] = cum[edge:edge + 1, :]
+
+    for p in range(pieces):
+        cross(tp, p, 0).wait_send()
+        remote(rows_piece(sibling, p), rows_piece(sibling, p), s.cs.at[p], s.cr.at[p],
+               "tp", sibling).wait_recv()
+    project_chip(x)
+    for chunk in key_chunks:
+        if sp_count > 2:
+            z_arrive(1, chunk)
+    decay_chip(x)
+    for chunk in query_chunks:
+        z_arrive(0, chunk, False)
     ctx_low = dot(s.mod_context[...], s.low_w[...], ((1,), (1,))).astype(bf16)
     ctx_totals = []
     for direction in range(2):
@@ -790,58 +831,32 @@
         ctx_totals.append(cum[edge:edge + 1, :])
         s.ctx_close[direction] = jnp.exp(ctx_totals[direction] - cum)
     s.ctx_value[...] = dot(s.mod_context[...], s.value_w[...]).astype(bf16)
-    load_gate_w.wait()
-
-    def project_chip(chip):
-        rows = pl.ds(pl.multiple_of(chip * 2 * own, 2 * own), 2 * own)
-        mod = (s.rows[rows, :].astype(f32) * s.scales[0:1, :]
-               + s.shifts[0:1, :]).astype(bf16)
-        s.mod_latent[rows, :] = mod
-        s.low[rows, :] = dot(mod, s.low_w[...], ((1,), (1,))).astype(bf16)
-        s.value[rows, :] = dot(mod, s.value_w[...]).astype(bf16)
-        s.gate[rows, :] = dot(mod, s.gate_w[...]).astype(bf16)
-
-    for chunk in key_chunks:
-        if sp_count > 2:
-            z_arrive(1, chunk)
-    for p in range(pieces):
-        cross(tp, p, 0).wait_send()
-        remote(rows_piece(sibling, p), rows_piece(sibling, p), s.cs.at[p], s.cr.at[p],
-               "tp", sibling).wait_recv()
-    project_chip(x)
+    for hop in range(2, sp_count - 1):
+        for chunk in key_chunks:
+            z_arrive(hop, chunk)
     for chunk in query_chunks:
-        z_arrive(0, chunk)
+        y_each(0, chunk, weight_view(grp), lambda c: c.start())
     for p in range(pieces):
         x_copy(across, p).wait_recv()
         cross(across, p, 1).start()
-    for hop in range(2, sp_count - 1):
-        for chunk in key_chunks:
-            z_arrive(hop, chunk)
+    if sp_count > 2:
+        for chunk in query_chunks:
+            z_arrive(1, chunk)
     for p in range(pieces):
         cross(far_sibling, p, 1).wait_recv()
     project_chip(1 - x)
-
-    own_head = lax.broadcasted_iota(jnp.int32, (ATTENTION_HEADS, size), 0) == tp
+    decay_chip(1 - x)
     for direction in range(2):
-        mask = triangle(size, direction == 1).astype(f32)
-        edge = 0 if direction == 1 else size - 1
         before = None
         for turn in range(blocks):
             b = blocks - 1 - turn if direction == 1 else turn
-            rows = slice(b * size, (b + 1) * size)
-            head_extra = jnp.sum(jnp.where(own_head, s.extra[direction, :, rows], 0.0), axis=0,
-                                 keepdims=True)
-            added = jnp.sum(mask * head_extra, axis=1, keepdims=True)
-            cum = dot(mask, decay_of(s.low[rows, :], direction), precision=highest) + added
-            s.cum[direction, rows, :] = cum
-            block_total = cum[edge:edge + 1, :]
             if before is not None:
                 s.ahead[direction, b:b + 1, :] = before
+            block_total = s.block_total[direction, b]
             before = block_total if before is None else before + block_total
         s.total[direction:direction + 1, :] = before
     s.totals[sp] = jnp.concatenate([s.total[...]] + ctx_totals, axis=0)
     tot_go()
-
     for hop in range(sp_count - 1):
         for chunk in key_chunks:
             y_each(hop, chunk, other_view, lambda c: c.wait_recv())
@@ -853,9 +868,6 @@
         rows = slice(b * size, (b + 1) * size)
         key = dot(s.mod_latent[rows, :], s.wqk[0]).astype(bf16)
         s.key[rows, :] = rotate(key.astype(f32), s.cosine[rows, :], s.sine[rows, :])
-    if sp_count > 2:
-        for chunk in query_chunks:
-            z_arrive(1, chunk)
     for direction in range(2):
         edge = 0 if direction == 1 else size - 1
         state = None
@@ -874,7 +886,8 @@
         s.state[direction] = state
     tot_arrive()
     chunk_width = s.chain_in.shape[3]
-    chunk_count = s.chain_in.shape[1]
+    chunk_count = vals // chunk_width
+    steps = s.chain_in.shape[1]
 
     def column(row):
         return jnp.broadcast_to(jnp.exp(row).T, (keys, chunk_width))
@@ -899,13 +912,17 @@
                 s.own_decay[direction] * s.ahead_decay[direction] * carried)
 
     first_way = jnp.where(sp < sp_count // 2, 0, 1)
-
-    def chain_copy(way, c, target):
-        return remote(s.chain_out.at[way, c], s.chain_in.at[way, c], s.hs.at[way, c],
-                      s.hr.at[way, c], "sp", target)
-
-    def chain(way, c, sources):
+    halves = keys // s.chain_in.shape[2] * 2
+    part_keys = keys // halves
+
+    def chain_copy(way, i, target):
+        return remote(s.chain_out.at[way, i], s.chain_in.at[way, i], s.hs.at[way, i],
+                      s.hr.at[way, i], "sp", target)
+
+    def chain(way, i, sources):
+        c, part = i // halves, i % halves
         cols = slice(c * chunk_width, (c + 1) * chunk_width)
+        rows = slice(part * part_keys, (part + 1) * part_keys)
         onward = 1 - 2 * way
         has_before = jnp.where(way == 0, sp > 0, sp < sp_count - 1)
         has_next = jnp.where(way == 0, sp < sp_count - 1, sp > 0)
@@ -913,17 +930,17 @@
         @pl.when(jnp.logical_and(has_next, jnp.logical_not(has_before)) if sources else has_before)
         def _():
             if not sources:
-                chain_copy(way, c, sp - onward).wait_recv()
+                chain_copy(way, i, sp - onward).wait_recv()
 
             @pl.when(has_next)
             def _():
-                s.chain_out[way, c, :keys, :] = (
-                    s.own_decay[way] * s.chain_in[way, c, :keys, :].astype(f32)
-                    + s.state[way, :, cols]).astype(bf16)
-                s.chain_out[way, c, keys:, :] = (
-                    s.chain_in[way, c, keys:, :].astype(f32)
-                    + s.carry[1 - way, :, cols]).astype(bf16)
-                chain_copy(way, c, sp + onward).start()
+                s.chain_out[way, i, :part_keys, :] = (
+                    s.own_decay[way, rows, :] * s.chain_in[way, i, :part_keys, :].astype(f32)
+                    + s.state[way, rows, cols]).astype(bf16)
+                s.chain_out[way, i, part_keys:, :] = (
+                    s.chain_in[way, i, part_keys:, :].astype(f32)
+                    + s.carry[1 - way, rows, cols]).astype(bf16)
+                chain_copy(way, i, sp + onward).start()
 
     def attend(b):
         rows = slice(b * size, (b + 1) * size)
@@ -950,29 +967,37 @@
         inner = dot(scores.astype(bf16), s.value[rows, :])
         s.mixture[rows, :] = inner if out is None else out + inner
 
-    for c in range(chunk_count):
-        chain(first_way, c, True)
+    for i in range(steps):
+        chain(first_way, i, True)
     for hop in range(2, sp_count - 1):
         for chunk in query_chunks:
             z_arrive(hop, chunk)
+    load_gate_w.wait()
+    gate_chip(x)
+    gate_chip(1 - x)
     for hop in range(sp_count - 1):
         for chunk in query_chunks:
             y_each(hop, chunk, other_view, lambda c: c.wait_recv())
-    for turn in range(max(blocks, chunk_count)):
+    lag = 2
+    for turn in range(max(blocks, steps + lag)):
         if turn < blocks:
             attend(turn)
-        if turn < chunk_count:
+        if turn < steps:
             chain(first_way, turn, False)
-    for c in range(chunk_count):
-        chain(1 - first_way, c, False)
+        if turn >= lag:
+            chain(1 - first_way, turn - lag, False)
     for c in range(chunk_count):
         cols = slice(c * chunk_width, (c + 1) * chunk_width)
-        for direction in range(2):
-            joined = (s.chain_in[direction, c, :keys, :].astype(f32)
-                      + s.ahead_decay[direction]
-                      * (s.carry[direction, :, cols]
-                         + s.chain_in[1 - direction, c, keys:, :].astype(f32)))
-            s.joined[direction * keys:(direction + 1) * keys, cols] = joined.astype(bf16)
+        for part in range(halves):
+            i = c * halves + part
+            rows = slice(part * part_keys, (part + 1) * part_keys)
+            for direction in range(2):
+                joined = (s.chain_in[direction, i, :part_keys, :].astype(f32)
+                          + s.ahead_decay[direction, rows, :]
+                          * (s.carry[direction, rows, cols]
+                             + s.chain_in[1 - direction, i, part_keys:, :].astype(f32)))
+                start = direction * keys + part * part_keys
+                s.joined[start:start + part_keys, cols] = joined.astype(bf16)
     for load in (load_norm_gain, load_out_w, load_final_gain, load_final_bias):
         load.wait()
 
@@ -1044,8 +1069,8 @@
 
         @pl.when(has_next)
         def _():
-            for c in range(chunk_count):
-                chain_copy(way, c, sp + 1 if way == 0 else sp - 1).wait_send()
+            for i in range(steps):
+                chain_copy(way, i, sp + 1 if way == 0 else sp - 1).wait_send()
     for n in range(out_chunks):
         pair_copy(0, n).wait_send()
         pair_copy(1, n).wait_send()
@@ -1107,14 +1132,15 @@
         key=vmem((count, keys), f32),
         cum=vmem((2, count, keys), f32),
         ahead=vmem((2, blocks, keys), f32),
+        block_total=vmem((2, blocks, 1, keys), f32),
         total=vmem((2, keys), f32),
         start=vmem((2, blocks, keys, vals), bf16),
         state=vmem((2, keys, vals), f32),
         carry=vmem((2, keys, vals), f32),
         own_decay=vmem((2, keys, vals // chains), f32),
         ahead_decay=vmem((2, keys, vals // chains), f32),
-        chain_in=vmem((2, chains, 2 * keys, vals // chains), bf16),
-        chain_out=vmem((2, chains, 2 * keys, vals // chains), bf16),
+        chain_in=vmem((2, 2 * chains, keys, vals // chains), bf16),
+        chain_out=vmem((2, 2 * chains, keys, vals // chains), bf16),
         q_all=vmem((count, 2 * keys), bf16),
         mixture=vmem((count, vals), f32),
         joined=vmem((2 * keys, vals), bf16),
@@ -1131,7 +1157,7 @@
         cs=dma((2 * pieces,)), cr=dma((2 * pieces,)),
         ps=dma((hops,)), pr=dma((hops,)), ts=dma((hops,)), tr=dma((hops,)),
         ss=dma((tp_count - 1,)), sr=dma((tp_count - 1,)),
-        hs=dma((2, chains)), hr=dma((2, chains)),
+        hs=dma((2, 2 * chains)), hr=dma((2, 2 * chains)),
         ds=dma((2, outs)), dr=dma((2, outs)), fs=dma((outs,)), fr=dma((outs,)),
     )
     return pl.pallas_call(

time: 75.5 us -> 69.3 us (0.918)
  Pallas kernels: 73.4 us -> 67.2 us
    pallas_call x1, Pallas kernels: 73.4 us -> 67.2 us  [fused(): pl.pallas_call(fused_kernel, out_shape=jax.ShapeDtypeStruct((own, width),...]
where the time goes in v2:
time: 69.3 us; the launch traced here: 69.1 us
  Pallas kernels  67.2 us (97%)
  local copies, waits for them, and re-layouts  1.88 us (3%)
    pallas_call x1, Pallas kernels, fused(): pl.pallas_call(fused_kernel, out_shape=jax.ShapeDtypeStruct((own, width),...  67.2 us
    unnamed x1, local copies, waits for them, and re-layouts  1.88 us

profile of v2, /device:TPU:0, one launch (start us, length us, event | category | flops | bytes accessed | tf_op | source)
XLA Modules:
  0.0 69.1 jit_solution(3704581214660281158)
XLA Ops:
  0.0 67.2 %shard_map.172 = bf16[128,2048]{1,0:T(8,128)(2,1)} custom-call(bf16[128,2048]{1,0:T(8,128)(2,1)} %latent.1, bf16[128,2048]{1,0:T(8,128)(2,1)} %context.1, f32[1,512]{1,0:T(1,128)} %bitcast.11, f32[1,512]{1,0:T(1,128)} %bitcast.12, bf16[512,1536]{1,0:T(8,128)(2,1)} %mod_w.1, f32[1,6144]{1,0:T(1,128)} %bitcast.8, bf16[512,1024]{1,0:T(8,128)(2,1)} %query_w.1, ...), custom_call_target="tpu_custom_call" | custom-call | flops 6000000000 | bytes 12000000 | tf_op jit(solution)/shard_map/pallas_call | solution.py:1163
  67.2 1.9 %copy.20 = bf16[128,2048]{1,0:T(8,128)(2,1)} copy(bf16[128,2048]{1,0:T(8,128)(2,1)} %shard_map.172) | data formatting | bytes 1048576

commit v3 on v2

--- a/solution.py
+++ b/solution.py
@@ -542,6 +542,7 @@
     part: Any
     sums: Any
     totals: Any
+    ctx_totals: Any
     shifts: Any
     scales: Any
     branch_gate: Any
@@ -568,10 +569,7 @@
     mixture: Any
     joined: Any
     gated: Any
-    pair_out: Any
-    pair_in: Any
-    far_out: Any
-    far_in: Any
+    gathered: Any
     branch: Any
     load_sem: Any
     zs: Any
@@ -582,18 +580,26 @@
     xr: Any
     cs: Any
     cr: Any
+    ocs: Any
+    ocr: Any
+    ods: Any
+    odr: Any
+    oxs: Any
+    oxr: Any
+    oys: Any
+    oyr: Any
+    gs: Any
+    gr: Any
     ps: Any
     pr: Any
     ts: Any
     tr: Any
+    us: Any
+    ur: Any
     ss: Any
     sr: Any
     hs: Any
     hr: Any
-    ds: Any
-    dr: Any
-    fs: Any
-    fr: Any
 
 
 def spread_of(ref, axis, send_sem, recv_sem):
@@ -602,7 +608,25 @@
             lambda: spread_drain(ref, axis, send_sem, recv_sem))
 
 
-PARTS = 2
+class SharedLine(Line):
+    def copy(self, way, hop, chunk, block, target):
+        ref = self.view(block, chunk)
+        return remote(ref, ref, self.send_sem.at[way, hop], self.recv_sem.at[way, hop, chunk],
+                      self.axis, self.target_of(target))
+
+    def drain_whole(self, whole):
+        for way in range(2):
+            for hop in range(self.count - 1):
+                block, target, valid = self.outgoing(way, hop)
+
+                @pl.when(valid)
+                def _():
+                    remote(whole, whole, self.send_sem.at[way, hop],
+                           self.recv_sem.at[way, hop, 0], self.axis,
+                           self.target_of(target)).wait_send()
+
+
+PARTS = 4
 
 
 def fused_kernel(latent, context, cond, ctx_cond, mod_w, mod_b, query_w, key_w, value_w, gate_w,
@@ -632,22 +656,21 @@
     own_depth = pl.ds(pl.multiple_of(sp * depth, depth), depth)
     loads = []
     for i, (source, target) in enumerate((
-        (cond, s.cond), (ctx_cond, s.ctx_cond),
-        (mod_w, s.mod_w),
+        (latent, s.rows.at[block_rows(tp), :]),
+        (cond, s.cond), (ctx_cond, s.ctx_cond), (mod_w, s.mod_w),
         (key_w.at[:, head_cols], s.wqk.at[0, own_depth, :]),
         (query_w.at[:, head_cols], s.wqk.at[1, own_depth, :]),
-        (latent, s.rows.at[block_rows(tp), :]),
         (mod_b, s.mod_b), (context, s.context),
         (low_w, s.low_w), (value_w, s.value_w),
         (decay_w.at[:, :, head_cols], s.decay_w),
         (decay_b.at[:, head_cols], s.decay_b), (extra, s.extra),
         (gate_w, s.gate_w), (norm_gain, s.norm_gain),
-        (out_w, s.out_w), (final_gain, s.final_gain),
+        (out_w, s.out_w.at[tp]), (final_gain, s.final_gain),
         (final_bias, s.final_bias),
     )):
         loads.append(pltpu.make_async_copy(source, target, s.load_sem.at[i]))
         loads[i].start()
-    (load_cond, load_ctx_cond, load_mod_w, load_key_w, load_query_w, load_latent,
+    (load_latent, load_cond, load_ctx_cond, load_mod_w, load_key_w, load_query_w,
      load_mod_b, load_context, load_low_w, load_value_w, load_decay_w, load_decay_b,
      load_extra, load_gate_w, load_norm_gain, load_out_w, load_final_gain, load_final_bias) = loads
 
@@ -660,28 +683,43 @@
             return s.wqk.at[chunk // PARTS, pl.ds(pl.multiple_of(start, step), step), :]
         return view
 
-    line = Line(sp, sp_count, "sp", lambda p: p, weight_view(grp), 2 * PARTS, s.zs, s.zr)
-    other_view = weight_view(1 - grp)
-
-    def y_copy(ref, way, hop, chunk):
-        return remote(ref, ref, s.ys.at[way, hop, chunk], s.yr.at[way, hop, chunk],
-                      "grp", 1 - grp)
+    line = SharedLine(sp, sp_count, "sp", lambda p: p, weight_view(grp), 2 * PARTS, s.zs, s.zr)
+
+    def y_copy(ref, way, hop, matrix):
+        return remote(ref, ref, s.ys.at[way, hop], s.yr.at[way, hop, matrix], "grp", 1 - grp)
 
     def z_arrive(hop, chunk, pass_on=True):
         for way in range(2):
             line.arrive(way, hop, chunk, (lambda block: y_copy(
-                weight_view(grp)(block, chunk), way, hop, chunk).start()) if pass_on else None)
+                weight_view(grp)(block, chunk), way, hop, chunk // PARTS).start()) if pass_on else None)
             if hop + 1 < sp_count - 1:
                 line.send(way, hop + 1, chunk)
 
-    def y_each(hop, chunk, view, act):
+    def y_each(hop, act):
         for way in range(2):
             block = sp - 1 - hop if way == 0 else sp + 1 + hop
             valid = sp > hop if way == 0 else sp + 1 + hop < sp_count
 
             @pl.when(valid)
             def _():
-                act(y_copy(view(block, chunk), way, hop, chunk))
+                act(block, way)
+
+    def y_start(hop, chunk):
+        y_each(hop, lambda block, way: y_copy(
+            weight_view(grp)(block, chunk), way, hop, chunk // PARTS).start())
+
+    def y_arrive(matrix):
+        def wait(hop, block, way):
+            start = pl.multiple_of(block * depth + (1 - grp) * half, half)
+            y_copy(s.wqk.at[matrix, pl.ds(start, half), :], way, hop, matrix).wait_recv()
+
+        for hop in range(sp_count - 1):
+            y_each(hop, functools.partial(wait, hop))
+
+    def y_drain():
+        whole = s.wqk.at[0, pl.ds(0, depth), :]
+        for hop in range(sp_count - 1):
+            y_each(hop, lambda block, way: y_copy(whole, way, hop, 0).wait_send())
 
     key_chunks, query_chunks = range(PARTS), range(PARTS, 2 * PARTS)
 
@@ -690,41 +728,87 @@
             for way in range(2):
                 line.send(way, 0, chunk)
 
-    pieces, early = s.xs.shape[0], 1
+    pieces, early = s.xr.shape[0], 3
     piece = own // pieces
 
     def rows_piece(j, p):
         return s.rows.at[pl.ds(pl.multiple_of(j * own + p * piece, piece), piece), :]
 
     def x_copy(j, p):
-        return remote(rows_piece(j, p), rows_piece(j, p), s.xs.at[p], s.xr.at[p],
+        return remote(rows_piece(j, p), rows_piece(j, p), s.xs.at[0], s.xr.at[p],
                       "tp", across)
 
     def cross(j, p, slot):
-        k = slot * pieces + p
-        return remote(rows_piece(j, p), rows_piece(j, p), s.cs.at[k], s.cr.at[k],
+        return remote(rows_piece(j, p), rows_piece(j, p), s.cs.at[slot], s.cr.at[slot],
                       "tp", sibling)
+
+    def cross_whole(j, slot):
+        ref = s.rows.at[block_rows(j), :]
+        return remote(ref, ref, s.cs.at[slot], s.cr.at[slot], "tp", sibling)
+
+    out_rows = s.out_w.shape[1]
+    out_half = out_rows // 2
+    out_pieces = s.oyr.shape[0]
+    out_step = out_half // out_pieces
+
+    direct = out_pieces // 4
+    shared = out_pieces - direct
+
+    def out_piece(j, side, p):
+        start = pl.multiple_of(side * out_half + p * out_step, out_step)
+        return s.out_w.at[j, pl.ds(start, out_step), :]
+
+    def out_bytes(count):
+        return s.out_w.at[tp, pl.ds(0, count * out_step), :]
+
+    def out_own_copy(j=tp):
+        return remote(s.out_w.at[j], s.out_w.at[j], s.ocs.at[0], s.ocr.at[0], "tp", sibling)
+
+    def out_x(j, k):
+        side, p = (grp, k) if k < out_pieces else (1 - grp, shared + k - out_pieces)
+        ref = out_piece(j, side, p)
+        return remote(ref, ref, s.oxs.at[0], s.oxr.at[k], "tp", across)
+
+    def out_y(side, p):
+        ref = out_piece(across, side, p)
+        return remote(ref, ref, s.oys.at[0], s.oyr.at[p], "grp", 1 - grp)
+
+    def out_pass(ref, way):
+        return remote(ref, ref, s.ods.at[way], s.odr.at[way], "tp", sibling)
+
+    def relay_x(k):
+        copy = out_x(across, k)
+        copy.wait_recv()
+        if k < shared:
+            out_y(grp, k).start()
+        side, p = (grp, k) if k < out_pieces else (1 - grp, shared + k - out_pieces)
+        out_pass(out_piece(across, side, p), 0).start()
+
+    def relay_y(p):
+        out_y(1 - grp, p).wait_recv()
+        out_pass(out_piece(across, 1 - grp, p), 1).start()
 
     part_go, part_arrive, part_drain = spread_of(s.part, "sp", s.ps, s.pr)
     sums_go, sums_arrive, sums_drain = spread_of(s.sums, "tp", s.ss, s.sr)
     tot_go, tot_arrive, tot_drain = spread_of(s.totals, "sp", s.ts, s.tr)
-
+    ctx_go, ctx_arrive, ctx_drain = spread_of(s.ctx_totals, "sp", s.us, s.ur)
+
+    load_latent.wait()
+    ready()
+    for p in range(pieces):
+        if p < early:
+            x_copy(tp, p).start()
+        cross(tp, p, 0).start()
     for load in (load_cond, load_ctx_cond, load_mod_w):
         load.wait()
     v = jnp.concatenate([s.cond[...], s.ctx_cond[...]], axis=0)
     activated = (v / (1.0 + jnp.exp(-v))).astype(bf16)
     s.part[sp] = dot(activated, s.mod_w[...])
-    for load in (load_key_w, load_query_w, load_latent):
-        load.wait()
-
-    ready()
     part_go()
+    load_key_w.wait()
+    load_query_w.wait()
     send_own(key_chunks)
-    send_own(query_chunks[:1])
-    for p in range(pieces):
-        if p < early:
-            x_copy(tp, p).start()
-        cross(tp, p, 0).start()
+    send_own(query_chunks[:PARTS // 2])
 
     quarter = keys // 4
 
@@ -763,9 +847,13 @@
     sums_go()
     for p in range(early, pieces):
         x_copy(tp, p).start()
+    load_out_w.wait()
+    out_own_copy().start()
+    for k in range(out_pieces + direct):
+        out_x(tp, k).start()
     for chunk in key_chunks:
         z_arrive(0, chunk)
-    send_own(query_chunks[1:])
+    send_own(query_chunks[PARTS // 2:])
     sums_arrive()
     for load in (load_mod_b, load_context, load_low_w, load_value_w, load_decay_w, load_decay_b, load_extra):
         load.wait()
@@ -811,17 +899,6 @@
                 s.cum[direction, rows, :] = cum
                 s.block_total[direction, b] = cum[edge:edge + 1, :]
 
-    for p in range(pieces):
-        cross(tp, p, 0).wait_send()
-        remote(rows_piece(sibling, p), rows_piece(sibling, p), s.cs.at[p], s.cr.at[p],
-               "tp", sibling).wait_recv()
-    project_chip(x)
-    for chunk in key_chunks:
-        if sp_count > 2:
-            z_arrive(1, chunk)
-    decay_chip(x)
-    for chunk in query_chunks:
-        z_arrive(0, chunk, False)
     ctx_low = dot(s.mod_context[...], s.low_w[...], ((1,), (1,))).astype(bf16)
     ctx_totals = []
     for direction in range(2):
@@ -830,21 +907,32 @@
         cum = dot(mask, decay_of(ctx_low, direction), precision=highest)
         ctx_totals.append(cum[edge:edge + 1, :])
         s.ctx_close[direction] = jnp.exp(ctx_totals[direction] - cum)
+    s.ctx_totals[sp] = jnp.concatenate(ctx_totals, axis=0)
+    ctx_go()
     s.ctx_value[...] = dot(s.mod_context[...], s.value_w[...]).astype(bf16)
+    for chunk in key_chunks:
+        if sp_count > 2:
+            z_arrive(1, chunk)
+    cross_whole(sibling, 0).wait_recv()
+    project_chip(x)
+    decay_chip(x)
+    for chunk in query_chunks:
+        z_arrive(0, chunk, False)
     for hop in range(2, sp_count - 1):
         for chunk in key_chunks:
             z_arrive(hop, chunk)
     for chunk in query_chunks:
-        y_each(0, chunk, weight_view(grp), lambda c: c.start())
+        y_start(0, chunk)
     for p in range(pieces):
         x_copy(across, p).wait_recv()
         cross(across, p, 1).start()
+    load_gate_w.wait()
+    gate_chip(x)
+    cross_whole(far_sibling, 1).wait_recv()
+    project_chip(1 - x)
     if sp_count > 2:
         for chunk in query_chunks:
             z_arrive(1, chunk)
-    for p in range(pieces):
-        cross(far_sibling, p, 1).wait_recv()
-    project_chip(1 - x)
     decay_chip(1 - x)
     for direction in range(2):
         before = None
@@ -855,15 +943,85 @@
             block_total = s.block_total[direction, b]
             before = block_total if before is None else before + block_total
         s.total[direction:direction + 1, :] = before
-    s.totals[sp] = jnp.concatenate([s.total[...]] + ctx_totals, axis=0)
+    s.totals[sp] = s.total[...]
     tot_go()
-    for hop in range(sp_count - 1):
-        for chunk in key_chunks:
-            y_each(hop, chunk, other_view, lambda c: c.wait_recv())
+    y_arrive(0)
+    chunk_width = s.chain_in.shape[4]
+    part_keys = s.chain_in.shape[3]
+    chunk_count = vals // chunk_width
+    turns_each = s.chain_in.shape[2]
+    steps = 2 * turns_each
+
+    def column(row):
+        return jnp.broadcast_to(jnp.exp(row).T, (keys, chunk_width))
+
+    def column_chunks():
+        return [slice(c * chunk_width, (c + 1) * chunk_width) for c in range(chunk_count)]
+
+    def sum_of(ref, direction, later):
+        total = jnp.zeros((1, keys), f32)
+        for j in range(sp_count):
+            chosen = (j > sp) if later else (j < sp)
+            total = total + jnp.where(chosen, ref[j, direction:direction + 1, :], 0.0)
+        return total
+
     ctx_key = dot(s.mod_context[...], s.wqk[0]).astype(bf16).astype(f32)
+    ctx_arrive()
     for direction in range(2):
         closing = (ctx_key * s.ctx_close[direction]).astype(bf16)
-        s.carry[direction] = dot(closing, s.ctx_value[...], ((0,), (0,)))
+        after = column(sum_of(s.ctx_totals, direction, direction == 0))
+        carry = dot(closing, s.ctx_value[...], ((0,), (0,)))
+        for cols in column_chunks():
+            s.carry[direction, :, cols] = after * carry[:, cols]
+    first_way = jnp.where(sp < sp_count // 2, 0, 1)
+
+    def ends(way):
+        return (jnp.where(way == 0, sp > 0, sp < sp_count - 1),
+                jnp.where(way == 0, sp < sp_count - 1, sp > 0))
+
+    def chain_copy(way, kind, c, target):
+        return remote(s.chain_out.at[way, kind, c], s.chain_in.at[way, kind, c],
+                      s.hs.at[way], s.hr.at[way, kind, c], "sp", target)
+
+    def chain_part(c):
+        part, col = c % (keys // part_keys), c // (keys // part_keys)
+        return (slice(part * part_keys, (part + 1) * part_keys),
+                slice(col * chunk_width, (col + 1) * chunk_width))
+
+    def chain_send(way, kind, c):
+        rows, cols = chain_part(c)
+        held = s.chain_in[way, kind, c].astype(f32)
+        if kind == 0:
+            added = held + s.carry[1 - way, rows, cols]
+        else:
+            added = s.own_decay[way, rows, :] * held + s.state[way, rows, cols]
+        s.chain_out[way, kind, c] = added.astype(bf16)
+        chain_copy(way, kind, c, sp + 1 - 2 * way).start()
+
+    def chain_open(way, kind):
+        has_before, has_next = ends(way)
+
+        @pl.when(jnp.logical_and(has_next, jnp.logical_not(has_before)))
+        def _():
+            if kind == 1:
+                for cols in column_chunks():
+                    s.state[way, :, cols] += s.own_decay[way] * s.carry[way, :, cols]
+            for c in range(turns_each):
+                chain_send(way, kind, c)
+
+    def chain(way, i):
+        kind, c = i // turns_each, i % turns_each
+        has_before, has_next = ends(way)
+
+        @pl.when(has_before)
+        def _():
+            chain_copy(way, kind, c, sp - 1 + 2 * way).wait_recv()
+
+            @pl.when(has_next)
+            def _():
+                chain_send(way, kind, c)
+
+    chain_open(first_way, 0)
     for b in range(blocks):
         rows = slice(b * size, (b + 1) * size)
         key = dot(s.mod_latent[rows, :], s.wqk[0]).astype(bf16)
@@ -884,63 +1042,19 @@
                 s.start[direction, b] = state.astype(bf16)
                 state = jnp.exp(block_total).T * state + term
         s.state[direction] = state
+    for direction in range(2):
+        s.own_decay[direction] = column(s.total[direction:direction + 1, :])
+    chain_open(first_way, 1)
+    relay_x(0)
     tot_arrive()
-    chunk_width = s.chain_in.shape[3]
-    chunk_count = vals // chunk_width
-    steps = s.chain_in.shape[1]
-
-    def column(row):
-        return jnp.broadcast_to(jnp.exp(row).T, (keys, chunk_width))
-
     for direction in range(2):
-        ahead = jnp.zeros((1, keys), f32)
-        after = jnp.zeros((1, keys), f32)
-        for j in range(sp_count):
-            upstream = (j > sp) if direction == 1 else (j < sp)
-            downstream = (j < sp) if direction == 1 else (j > sp)
-            ahead = ahead + jnp.where(upstream, s.totals[j, direction:direction + 1, :], 0.0)
-            after = after + jnp.where(
-                downstream, s.totals[j, 2 + direction:3 + direction, :], 0.0)
-        s.own_decay[direction] = column(s.total[direction:direction + 1, :])
-        s.ahead_decay[direction] = column(ahead)
-        after_decay = column(after)
-        for c in range(chunk_count):
-            cols = slice(c * chunk_width, (c + 1) * chunk_width)
-            carried = after_decay * s.carry[direction, :, cols]
-            s.carry[direction, :, cols] = carried
-            s.state[direction, :, cols] += (
-                s.own_decay[direction] * s.ahead_decay[direction] * carried)
-
-    first_way = jnp.where(sp < sp_count // 2, 0, 1)
-    halves = keys // s.chain_in.shape[2] * 2
-    part_keys = keys // halves
-
-    def chain_copy(way, i, target):
-        return remote(s.chain_out.at[way, i], s.chain_in.at[way, i], s.hs.at[way, i],
-                      s.hr.at[way, i], "sp", target)
-
-    def chain(way, i, sources):
-        c, part = i // halves, i % halves
-        cols = slice(c * chunk_width, (c + 1) * chunk_width)
-        rows = slice(part * part_keys, (part + 1) * part_keys)
-        onward = 1 - 2 * way
-        has_before = jnp.where(way == 0, sp > 0, sp < sp_count - 1)
-        has_next = jnp.where(way == 0, sp < sp_count - 1, sp > 0)
-
-        @pl.when(jnp.logical_and(has_next, jnp.logical_not(has_before)) if sources else has_before)
+        s.ahead_decay[direction] = column(sum_of(s.totals, direction, direction == 1))
+
+        @pl.when(ends(direction)[0])
         def _():
-            if not sources:
-                chain_copy(way, i, sp - onward).wait_recv()
-
-            @pl.when(has_next)
-            def _():
-                s.chain_out[way, i, :part_keys, :] = (
-                    s.own_decay[way, rows, :] * s.chain_in[way, i, :part_keys, :].astype(f32)
-                    + s.state[way, rows, cols]).astype(bf16)
-                s.chain_out[way, i, part_keys:, :] = (
-                    s.chain_in[way, i, part_keys:, :].astype(f32)
-                    + s.carry[1 - way, rows, cols]).astype(bf16)
-                chain_copy(way, i, sp + onward).start()
+            both = s.own_decay[direction] * s.ahead_decay[direction]
+            for cols in column_chunks():
+                s.state[direction, :, cols] += both * s.carry[direction, :, cols]
 
     def attend(b):
         rows = slice(b * size, (b + 1) * size)
@@ -967,87 +1081,86 @@
         inner = dot(scores.astype(bf16), s.value[rows, :])
         s.mixture[rows, :] = inner if out is None else out + inner
 
-    for i in range(steps):
-        chain(first_way, i, True)
+    lag, early_turns = 4, 8
+
+    def chain_turn(turn):
+        if turn < steps:
+            chain(first_way, turn)
+        if lag <= turn < steps + lag:
+            chain(1 - first_way, turn - lag)
+
+    for turn in range(lag):
+        chain_turn(turn)
     for hop in range(2, sp_count - 1):
         for chunk in query_chunks:
             z_arrive(hop, chunk)
-    load_gate_w.wait()
-    gate_chip(x)
+    for k in range(1, 3):
+        relay_x(k)
     gate_chip(1 - x)
-    for hop in range(sp_count - 1):
-        for chunk in query_chunks:
-            y_each(hop, chunk, other_view, lambda c: c.wait_recv())
-    lag = 2
-    for turn in range(max(blocks, steps + lag)):
-        if turn < blocks:
-            attend(turn)
-        if turn < steps:
-            chain(first_way, turn, False)
-        if turn >= lag:
-            chain(1 - first_way, turn - lag, False)
-    for c in range(chunk_count):
-        cols = slice(c * chunk_width, (c + 1) * chunk_width)
-        for part in range(halves):
-            i = c * halves + part
-            rows = slice(part * part_keys, (part + 1) * part_keys)
-            for direction in range(2):
-                joined = (s.chain_in[direction, i, :part_keys, :].astype(f32)
-                          + s.ahead_decay[direction, rows, :]
-                          * (s.carry[direction, rows, cols]
-                             + s.chain_in[1 - direction, i, part_keys:, :].astype(f32)))
-                start = direction * keys + part * part_keys
-                s.joined[start:start + part_keys, cols] = joined.astype(bf16)
-    for load in (load_norm_gain, load_out_w, load_final_gain, load_final_bias):
+    for turn in range(lag, early_turns):
+        chain_turn(turn)
+    y_arrive(1)
+    for turn in range(max(2 * blocks, steps + lag - early_turns)):
+        if turn % 2 == 0 and turn < 2 * blocks:
+            attend(turn // 2)
+        chain_turn(early_turns + turn)
+        if turn % 2 == 0 and 3 + turn // 2 < shared:
+            relay_x(3 + turn // 2)
+    for c in range(turns_each):
+        rows, cols = chain_part(c)
+        for direction in range(2):
+            joined = (s.chain_in[direction, 1, c].astype(f32)
+                      + s.ahead_decay[direction, rows, :]
+                      * (s.carry[direction, rows, cols]
+                         + s.chain_in[1 - direction, 0, c].astype(f32)))
+            start = direction * keys + rows.start
+            s.joined[start:start + part_keys, cols] = joined.astype(bf16)
+    for load in (load_norm_gain, load_final_gain, load_final_bias):
         load.wait()
 
-    def gate_rows(chip):
-        rows = pl.ds(pl.multiple_of(chip * 2 * own, 2 * own), 2 * own)
+    def gate_rows(j):
+        rows = block_rows(j)
         mixture = s.mixture[rows, :] + dot(s.q_all[rows, :], s.joined[...])
         squares = jnp.mean(mixture * mixture, axis=1, keepdims=True)
         gate = s.gate[rows, :].astype(f32)
         normed = mixture * lax.rsqrt(squares + norm_eps) * s.norm_gain[...]
         s.gated[rows, :] = (normed * (gate / (1.0 + jnp.exp(-gate)))).astype(bf16)
 
-    out_chunks = s.far_out.shape[0]
+    def gated_copy(k, j):
+        return remote(s.gated.at[block_rows(j), :], s.gathered.at[tp], s.gs.at[k], s.gr.at[k],
+                      "tp", j)
+
+    def gated_arrive(k, j):
+        remote(s.gathered.at[j], s.gathered.at[j], s.gs.at[k], s.gr.at[k], "tp", j).wait_recv()
+
+    out_chunks = 4
     out_width = width // out_chunks
-
-    def product(j, n):
-        cols = slice(n * out_width, (n + 1) * out_width)
-        return dot(s.gated[block_rows(j), :], s.out_w[:, cols])
-
-    def pair_copy(slot, n):
-        return remote(s.pair_out.at[slot, n], s.pair_in.at[slot, n], s.ds.at[slot, n],
-                      s.dr.at[slot, n], "tp", sibling)
-
-    def far_copy(n):
-        return remote(s.far_out.at[n], s.far_in.at[n], s.fs.at[n], s.fr.at[n],
-                      "tp", across)
-
-    gate_rows(1 - x)
-    for n in range(out_chunks):
-        s.pair_out[0, n] = product(far_sibling, n).astype(bf16)
-        pair_copy(0, n).start()
-    for n in range(out_chunks):
-        mine = product(across, n)
-        pair_copy(0, n).wait_recv()
-        s.far_out[n] = (mine + s.pair_in[0, n].astype(f32)).astype(bf16)
-        far_copy(n).start()
-    gate_rows(x)
-    for n in range(out_chunks):
-        s.pair_out[1, n] = product(sibling, n).astype(bf16)
-        pair_copy(1, n).start()
-    for n in range(out_chunks):
-        cols = slice(n * out_width, (n + 1) * out_width)
-        mine = product(tp, n)
-        pair_copy(1, n).wait_recv()
-        s.branch[:, cols] = mine + s.pair_in[1, n].astype(f32)
-    for n in range(out_chunks):
-        cols = slice(n * out_width, (n + 1) * out_width)
-        far_copy(n).wait_recv()
-        branch = s.branch[:, cols] + s.far_in[n].astype(f32)
+    out_cols = [slice(n * out_width, (n + 1) * out_width) for n in range(out_chunks)]
+
+    for k, j in ((1, across), (2, far_sibling), (0, sibling)):
+        gate_rows(j)
+        gated_copy(k, j).start()
+    gate_rows(tp)
+    for k in range(max(3, shared), out_pieces + direct):
+        relay_x(k)
+    for p in range(shared):
+        relay_y(p)
+    out_own_copy(sibling).wait_recv()
+    for cols in out_cols:
+        s.branch[:, cols] = dot(s.gated[block_rows(tp), :], s.out_w[tp, :, cols])
+    gated_arrive(0, sibling)
+    for cols in out_cols:
+        s.branch[:, cols] += dot(s.gathered[sibling], s.out_w[sibling, :, cols])
+    out_pass(out_bytes(out_pieces + direct), 0).wait_recv()
+    out_pass(out_bytes(shared), 1).wait_recv()
+    gated_arrive(1, across)
+    for cols in out_cols:
+        s.branch[:, cols] += dot(s.gathered[across], s.out_w[across, :, cols])
+    gated_arrive(2, far_sibling)
+    for cols in out_cols:
+        branch = s.branch[:, cols] + dot(s.gathered[far_sibling], s.out_w[far_sibling, :, cols])
         s.branch[:, cols] = (residual_scale * s.rows[block_rows(tp), cols].astype(f32)
-                                + s.branch_gate[:, cols] * branch)
+                             + s.branch_gate[:, cols] * branch)
     summed = s.branch[...]
     centered = summed - jnp.mean(summed, axis=1, keepdims=True)
     variance = jnp.mean(centered * centered, axis=1, keepdims=True)
@@ -1057,24 +1170,29 @@
     part_drain()
     sums_drain()
     tot_drain()
-    line.drain()
-    for hop in range(sp_count - 1):
-        for chunk in range(2 * PARTS):
-            y_each(hop, chunk, weight_view(grp), lambda c: c.wait_send())
-    for p in range(pieces):
-        x_copy(tp, p).wait_send()
-        cross(across, p, 1).wait_send()
+    ctx_drain()
+    line.drain_whole(s.wqk.at[0, pl.ds(0, depth), :])
+    y_drain()
+    own_rows = s.rows.at[block_rows(tp), :]
+    remote(own_rows, own_rows, s.xs.at[0], s.xr.at[0], "tp", across).wait_send()
+    for slot in range(2):
+        cross_whole(tp, slot).wait_send()
     for way in range(2):
         has_next = sp < sp_count - 1 if way == 0 else sp > 0
 
         @pl.when(has_next)
         def _():
-            for i in range(steps):
-                chain_copy(way, i, sp + 1 if way == 0 else sp - 1).wait_send()
-    for n in range(out_chunks):
-        pair_copy(0, n).wait_send()
-        pair_copy(1, n).wait_send()
-        far_copy(n).wait_send()
+            remote(s.chain_out.at[way], s.chain_in.at[way], s.hs.at[way], s.hr.at[way, 0, 0],
+                   "sp", sp + 1 - 2 * way).wait_send()
+    out_own_copy().wait_send()
+    ref = out_bytes(out_pieces + direct)
+    remote(ref, ref, s.oxs.at[0], s.oxr.at[0], "tp", across).wait_send()
+    out_pass(ref, 0).wait_send()
+    ref = out_bytes(shared)
+    remote(ref, ref, s.oys.at[0], s.oyr.at[0], "grp", 1 - grp).wait_send()
+    out_pass(ref, 1).wait_send()
+    for k, j in enumerate((sibling, across, far_sibling)):
+        gated_copy(k, j).wait_send()
 
 
 def fused(latent, context, condition, context_condition, mod_weight, mod_bias, query_weight,
@@ -1089,7 +1207,7 @@
     count = own * tp_count
     blocks = count // (2 * BLOCK)
     mod_cols = mod_weight.shape[1]
-    chains, outs, pieces = 4, 4, 4
+    chains, outs, pieces = 4, 8, 8
     args = (latent, context, condition[None, :], context_condition[None, :], mod_weight,
             mod_bias[None, :], query_weight, key_weight, value_weight, out_gate_weight,
             decay_in_weight.T, decay_weight, decay_bias, extra_decay, norm_gain[None, :],
@@ -1109,7 +1227,7 @@
         low_w=vmem(decay_in_weight.shape[::-1], bf16),
         value_w=vmem(value_weight.shape, bf16),
         gate_w=vmem(out_gate_weight.shape, bf16),
-        out_w=vmem(out_weight.shape, bf16),
+        out_w=vmem((tp_count,) + out_weight.shape, bf16),
         decay_w=vmem(decay_weight.shape[:2] + (keys,), bf16),
         decay_b=vmem((2, keys), f32),
         extra=vmem(extra_decay.shape, f32),
@@ -1118,7 +1236,8 @@
         final_bias=vmem((1, width), f32),
         part=vmem((sp_count, 2, mod_cols), f32),
         sums=vmem((tp_count, 2, mod_cols), f32),
-        totals=vmem((sp_count, 4, keys), f32),
+        totals=vmem((sp_count, 2, keys), f32),
+        ctx_totals=vmem((sp_count, 2, keys), f32),
         shifts=vmem((2, width), f32),
         scales=vmem((2, width), f32),
         branch_gate=vmem((1, width), f32),
@@ -1139,26 +1258,25 @@
         carry=vmem((2, keys, vals), f32),
         own_decay=vmem((2, keys, vals // chains), f32),
         ahead_decay=vmem((2, keys, vals // chains), f32),
-        chain_in=vmem((2, 2 * chains, keys, vals // chains), bf16),
-        chain_out=vmem((2, 2 * chains, keys, vals // chains), bf16),
+        chain_in=vmem((2, 2, 2 * chains, keys // 2, vals // chains), bf16),
+        chain_out=vmem((2, 2, 2 * chains, keys // 2, vals // chains), bf16),
         q_all=vmem((count, 2 * keys), bf16),
         mixture=vmem((count, vals), f32),
         joined=vmem((2 * keys, vals), bf16),
         gated=vmem((count, vals), bf16),
-        pair_out=vmem((2, outs, own, width // outs), bf16),
-        pair_in=vmem((2, outs, own, width // outs), bf16),
-        far_out=vmem((outs, own, width // outs), bf16),
-        far_in=vmem((outs, own, width // outs), bf16),
+        gathered=vmem((tp_count, own, vals), bf16),
         branch=vmem((own, width), f32),
         load_sem=dma((len(args),)),
-        zs=dma((2, hops, 2 * PARTS)), zr=dma((2, hops, 2 * PARTS)),
-        ys=dma((2, hops, 2 * PARTS)), yr=dma((2, hops, 2 * PARTS)),
-        xs=dma((pieces,)), xr=dma((pieces,)),
-        cs=dma((2 * pieces,)), cr=dma((2 * pieces,)),
+        zs=dma((2, hops)), zr=dma((2, hops, 2 * PARTS)),
+        ys=dma((2, hops)), yr=dma((2, hops, 2)),
+        xs=dma((1,)), xr=dma((pieces,)), cs=dma((2,)), cr=dma((2,)),
+        ocs=dma((1,)), ocr=dma((1,)), ods=dma((2,)), odr=dma((2,)),
+        oxs=dma((1,)), oxr=dma((outs + outs // 4,)), oys=dma((1,)), oyr=dma((outs,)),
+        gs=dma((tp_count - 1,)), gr=dma((tp_count - 1,)),
         ps=dma((hops,)), pr=dma((hops,)), ts=dma((hops,)), tr=dma((hops,)),
+        us=dma((hops,)), ur=dma((hops,)),
         ss=dma((tp_count - 1,)), sr=dma((tp_count - 1,)),
-        hs=dma((2, 2 * chains)), hr=dma((2, 2 * chains)),
-        ds=dma((2, outs)), dr=dma((2, outs)), fs=dma((outs,)), fr=dma((outs,)),
+        hs=dma((2,)), hr=dma((2, 2, 2 * chains)),
     )
     return pl.pallas_call(
         fused_kernel,

time: 69.3 us -> 57.2 us (0.83)
  Pallas kernels: 67.2 us -> 55.1 us
    pallas_call x1, Pallas kernels: 67.2 us -> 55.1 us  [fused(): pl.pallas_call(fused_kernel, out_shape=jax.ShapeDtypeStruct((own, width),...]
where the time goes in v3:
time: 57.2 us; the launch traced here: 57 us
  Pallas kernels  55.1 us (96%)
  local copies, waits for them, and re-layouts  1.88 us (3%)
    pallas_call x1, Pallas kernels, fused(): pl.pallas_call(fused_kernel, out_shape=jax.ShapeDtypeStruct((own, width),...  55.1 us
    unnamed x1, local copies, waits for them, and re-layouts  1.88 us

profile of v3, /device:TPU:0, one launch (start us, length us, event | category | flops | bytes accessed | tf_op | source)
XLA Modules:
  0.0 57.0 jit_solution(17169861191916014176)
XLA Ops:
  0.0 55.1 %shard_map.172 = bf16[128,2048]{1,0:T(8,128)(2,1)} custom-call(bf16[128,2048]{1,0:T(8,128)(2,1)} %latent.1, bf16[128,2048]{1,0:T(8,128)(2,1)} %context.1, f32[1,512]{1,0:T(1,128)} %bitcast.11, f32[1,512]{1,0:T(1,128)} %bitcast.12, bf16[512,1536]{1,0:T(8,128)(2,1)} %mod_w.1, f32[1,6144]{1,0:T(1,128)} %bitcast.8, bf16[512,1024]{1,0:T(8,128)(2,1)} %query_w.1, ...), custom_call_target="tpu_custom_call" | custom-call | flops 6000000000 | bytes 12000000 | tf_op jit(solution)/shard_map/pallas_call | solution.py:1281
  55.1 1.9 %copy.20 = bf16[128,2048]{1,0:T(8,128)(2,1)} copy(bf16[128,2048]{1,0:T(8,128)(2,1)} %shard_map.172) | data formatting | bytes 1048576

commit v4 on v3

--- a/solution.py
+++ b/solution.py
@@ -537,8 +537,6 @@
     decay_b: Any
     extra: Any
     norm_gain: Any
-    final_gain: Any
-    final_bias: Any
     part: Any
     sums: Any
     totals: Any
@@ -630,8 +628,7 @@
 
 
 def fused_kernel(latent, context, cond, ctx_cond, mod_w, mod_b, query_w, key_w, value_w, gate_w,
-                 low_w, decay_w, decay_b, extra, norm_gain, out_w, final_gain, final_bias,
-                 out_ref, s):
+                 low_w, decay_w, decay_b, extra, norm_gain, out_w, summed_ref, s):
     grp = lax.axis_index("grp")
     sp, sp_count = lax.axis_index("sp"), lax.axis_size("sp")
     tp, tp_count = lax.axis_index("tp"), lax.axis_size("tp")
@@ -665,14 +662,13 @@
         (decay_w.at[:, :, head_cols], s.decay_w),
         (decay_b.at[:, head_cols], s.decay_b), (extra, s.extra),
         (gate_w, s.gate_w), (norm_gain, s.norm_gain),
-        (out_w, s.out_w.at[tp]), (final_gain, s.final_gain),
-        (final_bias, s.final_bias),
+        (out_w, s.out_w.at[tp]),
     )):
         loads.append(pltpu.make_async_copy(source, target, s.load_sem.at[i]))
         loads[i].start()
     (load_latent, load_cond, load_ctx_cond, load_mod_w, load_key_w, load_query_w,
      load_mod_b, load_context, load_low_w, load_value_w, load_decay_w, load_decay_b,
-     load_extra, load_gate_w, load_norm_gain, load_out_w, load_final_gain, load_final_bias) = loads
+     load_extra, load_gate_w, load_norm_gain, load_out_w) = loads
 
     half = depth // 2
     step = half // PARTS
@@ -1115,8 +1111,7 @@
                          + s.chain_in[1 - direction, 0, c].astype(f32)))
             start = direction * keys + rows.start
             s.joined[start:start + part_keys, cols] = joined.astype(bf16)
-    for load in (load_norm_gain, load_final_gain, load_final_bias):
-        load.wait()
+    load_norm_gain.wait()
 
     def gate_rows(j):
         rows = block_rows(j)
@@ -1143,14 +1138,14 @@
     gate_rows(tp)
     for k in range(max(3, shared), out_pieces + direct):
         relay_x(k)
-    for p in range(shared):
-        relay_y(p)
     out_own_copy(sibling).wait_recv()
     for cols in out_cols:
         s.branch[:, cols] = dot(s.gated[block_rows(tp), :], s.out_w[tp, :, cols])
     gated_arrive(0, sibling)
     for cols in out_cols:
         s.branch[:, cols] += dot(s.gathered[sibling], s.out_w[sibling, :, cols])
+    for p in range(shared):
+        relay_y(p)
     out_pass(out_bytes(out_pieces + direct), 0).wait_recv()
     out_pass(out_bytes(shared), 1).wait_recv()
     gated_arrive(1, across)
@@ -1159,14 +1154,8 @@
     gated_arrive(2, far_sibling)
     for cols in out_cols:
         branch = s.branch[:, cols] + dot(s.gathered[far_sibling], s.out_w[far_sibling, :, cols])
-        s.branch[:, cols] = (residual_scale * s.rows[block_rows(tp), cols].astype(f32)
+        summed_ref[:, cols] = (residual_scale * s.rows[block_rows(tp), cols].astype(f32)
                              + s.branch_gate[:, cols] * branch)
-    summed = s.branch[...]
-    centered = summed - jnp.mean(summed, axis=1, keepdims=True)
-    variance = jnp.mean(centered * centered, axis=1, keepdims=True)
-    out_ref[...] = (centered * lax.rsqrt(variance + norm_eps) * s.final_gain[...]
-                    + s.final_bias[...]).astype(bf16)
-
     part_drain()
     sums_drain()
     tot_drain()
@@ -1193,6 +1182,14 @@
     out_pass(ref, 1).wait_send()
     for k, j in enumerate((sibling, across, far_sibling)):
         gated_copy(k, j).wait_send()
+
+
+def norm_kernel(summed_ref, gain_ref, bias_ref, out_ref):
+    summed = summed_ref[...]
+    centered = summed - jnp.mean(summed, axis=1, keepdims=True)
+    variance = jnp.mean(centered * centered, axis=1, keepdims=True)
+    out_ref[...] = (centered * lax.rsqrt(variance + norm_eps) * gain_ref[...]
+                    + bias_ref[...]).astype(bf16)
 
 
 def fused(latent, context, condition, context_condition, mod_weight, mod_bias, query_weight,
@@ -1211,7 +1208,7 @@
     args = (latent, context, condition[None, :], context_condition[None, :], mod_weight,
             mod_bias[None, :], query_weight, key_weight, value_weight, out_gate_weight,
             decay_in_weight.T, decay_weight, decay_bias, extra_decay, norm_gain[None, :],
-            out_weight, final_gain[None, :], final_bias[None, :])
+            out_weight)
     dma, vmem = pltpu.SemaphoreType.DMA, pltpu.VMEM
     hops = sp_count - 1
     scratch = Scratch(
@@ -1232,8 +1229,6 @@
         decay_b=vmem((2, keys), f32),
         extra=vmem(extra_decay.shape, f32),
         norm_gain=vmem((1, vals), f32),
-        final_gain=vmem((1, width), f32),
-        final_bias=vmem((1, width), f32),
         part=vmem((sp_count, 2, mod_cols), f32),
         sums=vmem((tp_count, 2, mod_cols), f32),
         totals=vmem((sp_count, 2, keys), f32),
@@ -1278,9 +1273,9 @@
         ss=dma((tp_count - 1,)), sr=dma((tp_count - 1,)),
         hs=dma((2,)), hr=dma((2, 2, 2 * chains)),
     )
-    return pl.pallas_call(
+    summed = pl.pallas_call(
         fused_kernel,
-        out_shape=jax.ShapeDtypeStruct((own, width), bf16),
+        out_shape=pltpu.VMEM((own, width), f32),
         in_specs=[pl.BlockSpec(memory_space=pltpu.HBM)] * len(args),
         out_specs=pl.BlockSpec(memory_space=pltpu.VMEM),
         scratch_shapes=[scratch],
@@ -1289,6 +1284,15 @@
         cost_estimate=pl.CostEstimate(flops=6_000_000_000, bytes_accessed=12_000_000,
                                       transcendentals=2_000_000),
     )(*args)
+    return pl.pallas_call(
+        norm_kernel,
+        out_shape=jax.ShapeDtypeStruct((own, width), bf16),
+        in_specs=[pl.BlockSpec(memory_space=pltpu.VMEM)] * 3,
+        out_specs=pl.BlockSpec(memory_space=pltpu.VMEM),
+        compiler_params=pltpu.CompilerParams(vmem_limit_bytes=8 * 1024 * 1024),
+        cost_estimate=pl.CostEstimate(flops=2_000_000, bytes_accessed=2_000_000,
+                                      transcendentals=1_000),
+    )(summed, final_gain[None, :], final_bias[None, :])
 
 
 def whole_heads(mesh):

time: 57.2 us -> 55.3 us (0.967)
  local copies, waits for them, and re-layouts: 1.88 us -> 0.01 us
    unnamed x1 -> x4, local copies, waits for them, and re-layouts: 1.88 us -> 0.01 us
    pallas_call x1 -> x2, Pallas kernels: 55.1 us -> 55 us  [the longest x1 53.8 us: fused(): pl.pallas_call(fused_kernel, out_shape=pltpu.VMEM((own, width), f32), in_...]
where the time goes in v4:
time: 55.3 us; the launch traced here: 55 us
  Pallas kernels  55 us (99%)
    pallas_call x1, Pallas kernels, fused(): pl.pallas_call(fused_kernel, out_shape=pltpu.VMEM((own, width), f32), in_...  53.8 us
    pallas_call x1, Pallas kernels, fused(): pl.pallas_call(norm_kernel, out_shape=jax.ShapeDtypeStruct((own, width),...  1.17 us

profile of v4, /device:TPU:0, one launch (start us, length us, event | category | flops | bytes accessed | tf_op | source)
XLA Modules:
  0.0 55.0 jit_solution(11725783915420479520)
XLA Ops:
  0.0 0.0 copy-start
  0.0 0.0 copy-start.1
  0.0 53.8 %shard_map.172.summed_ref = f32[128,2048]{1,0:T(8,128)S(1)} custom-call(bf16[128,2048]{1,0:T(8,128)(2,1)} %latent.1, bf16[128,2048]{1,0:T(8,128)(2,1)} %context.1, f32[1,512]{1,0:T(1,128)} %bitcast.11, f32[1,512]{1,0:T(1,128)} %bitcast.12, bf16[512,1536]{1,0:T(8,128)(2,1)} %mod_w.1, f32[1,6144]{1,0:T(1,128)} %bitcast.10, bf16[512,1024]{1,0:T(8,128)(2,1)} %query_w.1, ...), custom_call_target="tpu_custom_call" | custom-call | flops 6000000000 | bytes 12000000 | tf_op jit(solution)/shard_map/pallas_call | solution.py:1276
  53.9 0.0 copy-done
  53.9 0.0 copy-done.1
  53.9 1.2 %shard_map.173 = bf16[128,2048]{1,0:T(8,128)(2,1)} custom-call(f32[128,2048]{1,0:T(8,128)S(1)} %shard_map.172.summed_ref, f32[1,2048]{1,0:T(1,128)S(1)} %bitcast.7, f32[1,2048]{1,0:T(1,128)S(1)} %bitcast.8), custom_call_target="tpu_custom_call" | custom-call | flops 2000000 | bytes 2000000 | tf_op jit(solution)/shard_map/pallas_call | solution.py:1287
Async XLA Ops:
  0.0 53.9 %copy-start = (f32[2048]{0:T(1024)S(1)}, f32[2048]{0:T(1024)}, u32[]{:S(2)}) copy-start(f32[2048]{0:T(1024)} %param.34) | copy-start | bytes 24580
  0.0 53.9 %copy-start.1 = (f32[2048]{0:T(1024)S(1)}, f32[2048]{0:T(1024)}, u32[]{:S(2)}) copy-start(f32[2048]{0:T(1024)} %param.35) | copy-start | bytes 24580

commit v5 on v4

--- a/solution.py
+++ b/solution.py
@@ -1085,6 +1085,7 @@
         if lag <= turn < steps + lag:
             chain(1 - first_way, turn - lag)
 
+    gate_chip(1 - x)
     for turn in range(lag):
         chain_turn(turn)
     for hop in range(2, sp_count - 1):
@@ -1092,7 +1093,6 @@
             z_arrive(hop, chunk)
     for k in range(1, 3):
         relay_x(k)
-    gate_chip(1 - x)
     for turn in range(lag, early_turns):
         chain_turn(turn)
     y_arrive(1)

time: 55.3 us -> 55.3 us (level)
  no operation moved by 1% of the time
where the time goes in v5:
time: 55.3 us; the launch traced here: 55 us
  Pallas kernels  55 us (99%)
    pallas_call x1, Pallas kernels, fused(): pl.pallas_call(fused_kernel, out_shape=pltpu.VMEM((own, width), f32), in_...  53.8 us
    pallas_call x1, Pallas kernels, fused(): pl.pallas_call(norm_kernel, out_shape=jax.ShapeDtypeStruct((own, width),...  1.17 us

profile of v5, /device:TPU:0, one launch (start us, length us, event | category | flops | bytes accessed | tf_op | source)
XLA Modules:
  0.0 55.0 jit_solution(13479705015895298564)
XLA Ops:
  0.0 0.0 copy-start
  0.0 0.0 copy-start.1
  0.0 53.8 %shard_map.172.summed_ref = f32[128,2048]{1,0:T(8,128)S(1)} custom-call(bf16[128,2048]{1,0:T(8,128)(2,1)} %latent.1, bf16[128,2048]{1,0:T(8,128)(2,1)} %context.1, f32[1,512]{1,0:T(1,128)} %bitcast.11, f32[1,512]{1,0:T(1,128)} %bitcast.12, bf16[512,1536]{1,0:T(8,128)(2,1)} %mod_w.1, f32[1,6144]{1,0:T(1,128)} %bitcast.10, bf16[512,1024]{1,0:T(8,128)(2,1)} %query_w.1, ...), custom_call_target="tpu_custom_call" | custom-call | flops 6000000000 | bytes 12000000 | tf_op jit(solution)/shard_map/pallas_call | solution.py:1276
  53.8 0.0 copy-done
  53.8 0.0 copy-done.1
  53.8 1.2 %shard_map.173 = bf16[128,2048]{1,0:T(8,128)(2,1)} custom-call(f32[128,2048]{1,0:T(8,128)S(1)} %shard_map.172.summed_ref, f32[1,2048]{1,0:T(1,128)S(1)} %bitcast.7, f32[1,2048]{1,0:T(1,128)S(1)} %bitcast.8), custom_call_target="tpu_custom_call" | custom-call | flops 2000000 | bytes 2000000 | tf_op jit(solution)/shard_map/pallas_call | solution.py:1287
Async XLA Ops:
  0.0 53.8 %copy-start = (f32[2048]{0:T(1024)S(1)}, f32[2048]{0:T(1024)}, u32[]{:S(2)}) copy-start(f32[2048]{0:T(1024)} %param.34) | copy-start | bytes 24580
  0.0 53.8 %copy-start.1 = (f32[2048]{0:T(1024)S(1)}, f32[2048]{0:T(1024)}, u32[]{:S(2)}) copy-start(f32[2048]{0:T(1024)} %param.35) | copy-start | bytes 24580
